TPU v7x, 512 devices: a whole 4x4x16 slice. The times are simulated.
512 devices in a mesh: sp: 64 (over z, y), tp: 8 (over x, core).
Axes of the slice: x: 4, y: 4, z: 16, core: 2. Of those that a mesh axis runs over, the one named last changes fastest.
Arguments:
- tokens: bfloat16 [32768, 2048], P('sp', 'tp'), may hold values from -6 to 6
- norm_gain: float32 [2048], replicated, may hold values from 0.1 to 1.9
- outer_gate: bfloat16 [2048, 1024], P('sp', 'tp'), may hold values from -0.125 to 0.125
- inner_gate: bfloat16 [2048, 1024], P('sp', 'tp'), may hold values from -0.125 to 0.125
- conv_input: bfloat16 [2048, 1024], P('sp', 'tp'), may hold values from -0.125 to 0.125
- query_proj: bfloat16 [2048, 1024], P('sp', 'tp'), may hold values from -0.125 to 0.125
- key_proj: bfloat16 [2048, 1024], P('sp', 'tp'), may hold values from -0.125 to 0.125
- value_proj: bfloat16 [2048, 1024], P('sp', 'tp'), may hold values from -0.125 to 0.125
- out_gate: bfloat16 [2048, 1024], P('sp', 'tp'), may hold values from -0.125 to 0.125
- conv_taps: float32 [3, 1024], P(None, 'tp'), may hold values from -3.5 to 3.5
- log_decay: float32 [2, 16, 32768], P(None, 'tp', 'sp'), may hold values from -1.2 to 0, as said below
- head_gain: float32 [1024], P('tp'), may hold values from 0.1 to 1.9
- conv_output: bfloat16 [1024, 2048], P('tp', 'sp'), may hold values from -0.1875 to 0.1875
- retention_output: bfloat16 [1024, 2048], P('tp', 'sp'), may hold values from -0.1875 to 0.1875
Outputs:
- mixed: bfloat16 [32768, 2048], P(('sp', 'tp'))
Inputs may be any that keep to these rules, and one draw needn't show every extreme that they name: `log_decay`: logarithms of per-position decays, below zero.
All inputs are finite; a program needn't handle non-finite values.
Results may differ from a plain program's by a relative error of at most 0.02.
Values may be sent and summed in bfloat16 or wider, within the bound.
A program may use at most 128 MiB of HBM per device.

v0:
```python
import jax
import jax.numpy as jnp
from jax import lax
from jax.sharding import PartitionSpec as P

HEAD_DIM = 64


EPS = 1e-06
THETA = 10000.0


def with_halo(shard, sides, width):
    for axis, dim in sides:
        size, length = (lax.axis_size(axis), shard.shape[dim])
        up = [(i, (i + 1) % size) for i in range(size - 1)]
        down = [(j, i) for i, j in up]
        last = lax.slice_in_dim(shard, length - width, length, axis=dim)
        first = lax.slice_in_dim(shard, 0, width, axis=dim)
        before = lax.ppermute(last, axis, up)
        after = lax.ppermute(first, axis, down)
        shard = jnp.concatenate([before, shard, after], axis=dim)
    return shard


def from_everyone(shard, axis):
    copies = jnp.broadcast_to(shard, (lax.axis_size(axis), *shard.shape))
    return lax.all_to_all(copies, axis, split_axis=0, concat_axis=0, tiled=True)


def in_order(parts, dim):
    shape = list(parts.shape[1:])
    shape[dim] *= parts.shape[0]
    return jnp.moveaxis(parts, 0, dim).reshape(shape)


def collect(shard, axis, dim):
    parts = from_everyone(shard, axis)
    return in_order(parts, dim)


def in_one_piece(arrays, axis, dim, along):
    ends, at = ([], 0)
    for a in arrays[:-1]:
        at += a.shape[along]
        ends.append(at)
    both = jnp.concatenate(arrays, axis=along)
    return tuple(jnp.split(lax.all_gather(both, axis, axis=dim, tiled=True), ends, axis=along))


def turned_gather(arrays, axis, dims):
    turned = [jnp.moveaxis(a, dim, 0) for a, dim in zip(arrays, dims)]
    both = jnp.concatenate([t.reshape(len(t), -1) for t in turned], axis=1)
    filled, at, finished = (lax.all_gather(both, axis, axis=0, tiled=True), 0, [])
    for t, dim in zip(turned, dims):
        piece = filled[:, at : at + t[0].size].reshape(-1, *t.shape[1:])
        finished.append(jnp.moveaxis(piece, 0, dim))
        at += t[0].size
    return tuple(finished)


def in_blocks(shard, dim, size):
    before, after = (shard.shape[:dim], shard.shape[dim + 1 :])
    return jnp.moveaxis(shard.reshape(*before, size, -1, *after), dim, 0)


def sum_at_owner(shard, axis, dim):
    parts = in_blocks(shard, dim, lax.axis_size(axis))
    arrived = lax.all_to_all(parts, axis, split_axis=0, concat_axis=0, tiled=True)
    return arrived.astype(jnp.float32).sum(axis=0)


def rotate(field_in, position_list):
    half_dim = field_in.shape[-1] // 2
    frequency = jnp.exp(
        -jnp.log(THETA) * jnp.arange(half_dim, dtype=jnp.float32) * (2.0 / field_in.shape[-1])
    )
    angles = position_list.astype(jnp.float32)[:, None, None] * frequency
    cosine = jnp.cos(angles)
    sine_part = jnp.sin(angles)
    leading = field_in[..., :half_dim]
    trailing = field_in[..., half_dim:]
    return jnp.concatenate(
        [leading * cosine - trailing * sine_part, leading * sine_part + trailing * cosine], axis=-1
    )


def conv_branch(outer_rows, inner_rows, conv_values, conv_taps):
    inner_value = (inner_rows.astype(jnp.float32) * conv_values.astype(jnp.float32)).astype(
        jnp.bfloat16
    )
    padded = with_halo(inner_value, (("sp", 0),), 1).astype(jnp.float32)
    convolved = conv_taps[0] * padded[:-2] + conv_taps[1] * padded[1:-1] + conv_taps[2] * padded[2:]
    return (outer_rows.astype(jnp.float32) * convolved).astype(jnp.bfloat16)


def span_parts(query_rows, key_rows, value_rows, log_rates):
    length = query_rows.shape[0]
    forward_cum = jnp.cumsum(log_rates[0], axis=-1)
    backward_cum = jnp.flip(jnp.cumsum(jnp.flip(log_rates[1], -1), axis=-1), -1)
    row_index = lax.broadcasted_iota(jnp.int32, (length, length), 0)
    col_index = lax.broadcasted_iota(jnp.int32, (length, length), 1)
    lower_part = (col_index <= row_index)[None]
    spread = jnp.where(
        lower_part,
        forward_cum[:, :, None] - forward_cum[:, None, :],
        backward_cum[:, :, None] - backward_cum[:, None, :],
    )
    scores = jnp.einsum("ihe,jhe->hij", query_rows, key_rows, preferred_element_type=jnp.float32)
    weighted = (scores * jnp.exp(spread)).astype(jnp.bfloat16)
    local_part = jnp.einsum(
        "hij,jhe->ihe", weighted, value_rows, preferred_element_type=jnp.float32
    )
    key_wide = key_rows.astype(jnp.float32)
    forward_keys = (key_wide * jnp.exp(forward_cum[:, -1:] - forward_cum).T[:, :, None]).astype(
        jnp.bfloat16
    )
    backward_keys = (key_wide * jnp.exp(backward_cum[:, :1] - backward_cum).T[:, :, None]).astype(
        jnp.bfloat16
    )
    forward_state = jnp.einsum(
        "jhd,jhe->hde", forward_keys, value_rows, preferred_element_type=jnp.float32
    )
    backward_state = jnp.einsum(
        "jhd,jhe->hde", backward_keys, value_rows, preferred_element_type=jnp.float32
    )
    return (local_part, forward_cum, backward_cum, forward_state, backward_state)


def retention_branch(query_rows, key_rows, value_rows, gate_rows, log_decay, head_gain, offsets):
    row_count = query_rows.shape[0]
    head_count = query_rows.shape[1] // HEAD_DIM
    shape_heads = (row_count, head_count, HEAD_DIM)
    rotated_query = rotate(query_rows.astype(jnp.float32).reshape(shape_heads), offsets).astype(
        jnp.bfloat16
    )
    rotated_key = (
        rotate(key_rows.astype(jnp.float32).reshape(shape_heads), offsets) * HEAD_DIM ** (-0.5)
    ).astype(jnp.bfloat16)
    local_part, forward_cum, backward_cum, forward_state, backward_state = span_parts(
        rotated_query, rotated_key, value_rows.reshape(shape_heads), log_decay
    )
    forward_total = forward_cum[:, -1]
    backward_total = backward_cum[:, 0]
    totals = collect(jnp.stack([forward_total, backward_total])[None], "sp", 0)
    inclusive = jnp.cumsum(totals, axis=0)
    exclusive = inclusive - totals
    own_index = lax.axis_index("sp")
    own_inclusive = lax.dynamic_index_in_dim(inclusive, own_index, 0, keepdims=False)
    own_exclusive = lax.dynamic_index_in_dim(exclusive, own_index, 0, keepdims=False)
    pieces = in_one_piece((forward_state[None], backward_state[None]), "sp", 0, 1)
    piece_count = pieces[0].shape[0]
    span_index = lax.iota(jnp.int32, piece_count)
    forward_weight = jnp.where(
        (span_index < own_index)[:, None],
        jnp.exp(jnp.minimum(own_exclusive[0] - inclusive[:, 0], 0.0)),
        0.0,
    )
    backward_weight = jnp.where(
        (span_index > own_index)[:, None],
        jnp.exp(jnp.minimum(exclusive[:, 1] - own_inclusive[1], 0.0)),
        0.0,
    )
    into_forward = jnp.einsum("nh,nhde->hde", forward_weight, pieces[0])
    into_backward = jnp.einsum("nh,nhde->hde", backward_weight, pieces[1])
    forward_part = jnp.einsum(
        "ihd,hde->ihe",
        rotated_query,
        into_forward.astype(jnp.bfloat16),
        preferred_element_type=jnp.float32,
    )
    backward_part = jnp.einsum(
        "ihd,hde->ihe",
        rotated_query,
        into_backward.astype(jnp.bfloat16),
        preferred_element_type=jnp.float32,
    )
    mixed_heads = (
        local_part
        + jnp.exp(forward_cum).T[:, :, None] * forward_part
        + jnp.exp(backward_cum).T[:, :, None] * backward_part
    )
    scaled = mixed_heads * lax.rsqrt(
        jnp.mean(mixed_heads * mixed_heads, axis=-1, keepdims=True) + EPS
    )
    scaled = scaled * head_gain.reshape(head_count, HEAD_DIM)
    return (
        jax.nn.silu(gate_rows.astype(jnp.float32))
        * scaled.reshape(row_count, head_count * HEAD_DIM)
    ).astype(jnp.bfloat16)


def local(
    tokens,
    norm_gain,
    outer_gate,
    inner_gate,
    conv_input,
    query_proj,
    key_proj,
    value_proj,
    out_gate,
    conv_taps,
    log_decay,
    head_gain,
    conv_output,
    retention_output,
):
    whole = collect(tokens, "tp", 1)
    wide = whole.astype(jnp.float32)
    normed = (
        wide * lax.rsqrt(jnp.mean(wide * wide, axis=-1, keepdims=True) + EPS) * norm_gain
    ).astype(jnp.bfloat16)
    row_count = normed.shape[0]
    offsets = lax.axis_index("sp") * row_count + lax.iota(jnp.int32, row_count)
    gathered = turned_gather(
        (
            outer_gate,
            inner_gate,
            conv_input,
            query_proj,
            key_proj,
            value_proj,
            out_gate,
            conv_output,
            retention_output,
        ),
        "sp",
        (0, 0, 0, 0, 0, 0, 0, 1, 1),
    )
    projected = [
        jnp.dot(normed, weight, preferred_element_type=jnp.float32).astype(jnp.bfloat16)
        for weight in gathered[:7]
    ]
    conv_out = conv_branch(projected[0], projected[1], projected[2], conv_taps)
    ret_out = retention_branch(
        projected[3], projected[4], projected[5], projected[6], log_decay, head_gain, offsets
    )
    conv_weight = gathered[7]
    ret_weight = gathered[8]
    mixed = sum_at_owner(
        (
            jnp.dot(conv_out, conv_weight, preferred_element_type=jnp.float32)
            + jnp.dot(ret_out, ret_weight, preferred_element_type=jnp.float32)
        ).astype(jnp.bfloat16),
        "tp",
        0,
    )
    return mixed.astype(jnp.bfloat16)


def solution(mesh):
    return jax.shard_map(
        local,
        mesh=mesh,
        in_specs=(
            P("sp", "tp"),
            P(),
            P("sp", "tp"),
            P("sp", "tp"),
            P("sp", "tp"),
            P("sp", "tp"),
            P("sp", "tp"),
            P("sp", "tp"),
            P("sp", "tp"),
            P(None, "tp"),
            P(None, "tp", "sp"),
            P("tp"),
            P("tp", "sp"),
            P("tp", "sp"),
        ),
        out_specs=P(("sp", "tp"), None),
        check_vma=False,
    )
```

profile of v0, /device:TPU:1, one launch (start us, length us, event | category | flops | bytes accessed | tf_op | source)
XLA Modules:
  0.0 368.0 jit_solution(14018172722203421608)
XLA Ops:
  13.5 1.1 copy.26
  14.6 1.5 broadcast_in_dim.28
  16.2 10.5 %all-to-all-start = ((bf16[8,512,256]{1,2,0:T(8,128)(2,1)}), bf16[8,512,256]{1,2,0:T(8,128)(2,1)S(1)}, u32[]{:S(2)}, u32[]{:S(2)}) async-start(bf16[8,512,256]{1,2,0:T(8,128)(2,1)} %broadcast_in_dim.28), calls=%async_computation | async-start | bytes 4194304 | tf_op jit(solution)/shard_map/all_to_all | solution.py:28
  30.3 22.6 %all-to-all-done = bf16[8,512,256]{1,2,0:T(8,128)(2,1)S(1)} async-done(((bf16[8,512,256]{1,2,0:T(8,128)(2,1)}), bf16[8,512,256]{1,2,0:T(8,128)(2,1)S(1)}, u32[]{:S(2)}, u32[]{:S(2)}) %all-to-all-start) | async-done | bytes 2097184 | tf_op jit(solution)/shard_map/all_to_all | solution.py:28
  54.3 2.1 fusion.1
  56.4 100.9 %all-gather.3.cloned.1.call-done = bf16[2048,1152]{1,0:T(8,128)(2,1)} async-done(((bf16[32,1152]{1,0:T(8,128)(2,1)}), bf16[2048,1152]{1,0:T(8,128)(2,1)}) %all-gather.3.cloned.1.call-update) | async-done | bytes 4718608 | tf_op jit(solution)/shard_map/all_gather | solution.py:54
  157.3 1.5 convolution_convert_fusion
  158.8 1.5 convolution_convert_fusion.1
  160.5 1.5 convolution_convert_fusion.2
  163.8 9.0 %all-to-all-start.1 = ((f32[64,1,2,2]{3,2,1,0:T(2,128)}), f32[64,1,2,2]{3,2,1,0:T(2,128)S(1)}, u32[]{:S(2)}, u32[]{:S(2)}) async-start(f32[64,1,2,2]{3,2,1,0:T(2,128)} %broadcast_in_dim.35), calls=%async_computation.1 | async-start | bytes 131072 | tf_op jit(solution)/shard_map/all_to_all | solution.py:28
  173.0 13.8 %all-to-all-done.1 = f32[64,1,2,2]{3,2,1,0:T(2,128)S(1)} async-done(((f32[64,1,2,2]{3,2,1,0:T(2,128)}), f32[64,1,2,2]{3,2,1,0:T(2,128)S(1)}, u32[]{:S(2)}, u32[]{:S(2)}) %all-to-all-start.1) | async-done | bytes 1056 | tf_op jit(solution)/shard_map/all_to_all | solution.py:28
  187.3 1.8 fusion.16
  189.1 1.8 fusion.15
  190.9 2.1 collective-permute-start
  193.1 1.5 collective-permute-start.1
  195.6 2.2 collective-permute-done.1
  197.8 5.6 %fusion.20 = f32[512,2048]{1,0:T(8,128)} fusion(bf16[512,2048]{0,1:T(8,128)(2,1)S(1)} %fusion.1, bf16[2048,1152]{1,0:T(8,128)(2,1)} %all-gather.3.cloned.1.call-done, f32[514,128]{1,0:T(8,128)S(1)} %maximum_convert_fusion, f32[128]{0:T(128)S(1)} %get-tuple-element.24, f32[128]{0:T(128)S(1)} %get-tuple-element.25, f32[128]{0:T(128)S(1)} %get-tuple-element.23), kind=kOutput, calls=%fused_computation.33 | convolution fusion | flops 537460736 | bytes 8128000 | tf_op jit(solution)/shard_map/dot_general | solution.py:243
  203.4 100.5 %all-gather.5.cloned.1.call-done = bf16[64,4,64,64]{3,2,1,0:T(8,128)(2,1)} async-done(((bf16[1,4,64,64]{3,2,1,0:T(8,128)(2,1)}), bf16[64,4,64,64]{3,2,1,0:T(8,128)(2,1)}) %all-gather.5.cloned.1.call-update) | async-done | bytes 2097168 | tf_op jit(solution)/shard_map/all_gather | solution.py:48
  303.9 4.9 %fusion.72 = (bf16[64,2,64,64]{3,2,1,0:T(8,128)(2,1)S(1)}, bf16[64,2,64,64]{3,2,1,0:T(8,128)(2,1)}) fusion(bf16[64,4,64,64]{3,2,1,0:T(8,128)(2,1)} %all-gather.5.cloned.1.call-done), kind=kLoop, calls=%fused_computation.131 | loop fusion | bytes 4194304 | tf_op jit(solution)/shard_map/split | solution.py:48
  308.8 1.2 fusion.2
  310.2 2.8 fusion.4
  313.7 6.3 %add_convert_fusion = bf16[512,2048]{1,0:T(8,128)(2,1)} fusion(f32[512,2048]{1,0:T(8,128)} %fusion.20, bf16[2048,1152]{1,0:T(8,128)(2,1)} %all-gather.3.cloned.1.call-done, f32[512,128]{1,0:T(8,128)S(1)} %copy.31, bf16[512,2048]{0,1:T(8,128)(2,1)S(1)} %fusion.1), kind=kOutput, calls=%fused_computation.7 | convolution fusion | flops 539492352 | bytes 9699328 | tf_op jit(solution)/shard_map/dot_general | solution.py:244
  320.0 40.1 %all_to_all.15 = bf16[8,64,2048]{2,1,0:T(8,128)(2,1)S(1)} all-to-all(bf16[8,64,2048]{2,1,0:T(8,128)(2,1)} %bitcast.125), channel_id=1, replica_groups=mesh['sp'=64,'tp'=8] {'tp'}, dimensions={0} | all-to-all | bytes 4194304 | tf_op jit(solution)/shard_map/all_to_all | solution.py:69
  360.1 1.1 reduce_sum.32
  (84 shorter events, 16.3 us)
Async XLA Ops:
  6.5 150.7 %all-gather.3.cloned.1.call-start = ((), (), s32[]{:S(2)}) async-start(), calls=%async_computation.3 | async-start | bytes 4792320 | tf_op jit(solution)/shard_map/all_gather | solution.py:54
  12.9 0.6 copy-start.1
  16.2 10.5 %copy-start.3 = (f32[2,2,512]{2,1,0:T(2,128)S(1)}, f32[2,2,512]{2,1,0:T(2,128)}, u32[]{:S(2)}) copy-start(f32[2,2,512]{2,1,0:T(2,128)} %param.24) | copy-start | bytes 24580
  16.2 36.7 %all-to-all-start = ((bf16[8,512,256]{1,2,0:T(8,128)(2,1)}), bf16[8,512,256]{1,2,0:T(8,128)(2,1)S(1)}, u32[]{:S(2)}, u32[]{:S(2)}) async-start(bf16[8,512,256]{1,2,0:T(8,128)(2,1)} %broadcast_in_dim.28), calls=%async_computation | async-start | bytes 4194304 | tf_op jit(solution)/shard_map/all_to_all | solution.py:28
  26.6 27.6 %copy-start.2 = (f32[2048]{0:T(1024)S(1)}, f32[2048]{0:T(1024)}, u32[]{:S(2)}) copy-start(f32[2048]{0:T(1024)} %param.15) | copy-start | bytes 24580
  26.7 277.3 %all-gather.5.cloned.1.call-start = ((), (), s32[]{:S(2)}) async-start(), calls=%async_computation.4 | async-start | bytes 4259840 | tf_op jit(solution)/shard_map/all_gather | solution.py:48
  52.9 1.4 copy-start
  160.5 12.4 %copy-start.4 = (f32[3,128]{1,0:T(4,128)S(1)}, f32[3,128]{1,0:T(4,128)}, u32[]{:S(2)}) copy-start(f32[3,128]{1,0:T(4,128)} %param.23) | copy-start | bytes 4612
  160.5 12.4 %copy-start.5 = (f32[128]{0:T(128)S(1)}, f32[128]{0:T(128)}, u32[]{:S(2)}) copy-start(f32[128]{0:T(128)} %param.25) | copy-start | bytes 1540
  163.8 23.0 %all-to-all-start.1 = ((f32[64,1,2,2]{3,2,1,0:T(2,128)}), f32[64,1,2,2]{3,2,1,0:T(2,128)S(1)}, u32[]{:S(2)}, u32[]{:S(2)}) async-start(f32[64,1,2,2]{3,2,1,0:T(2,128)} %broadcast_in_dim.35), calls=%async_computation.1 | async-start | bytes 131072 | tf_op jit(solution)/shard_map/all_to_all | solution.py:28
  190.9 4.7 %collective-permute-start = (bf16[1,128]{1,0:T(2,128)(2,1)S(1)}, bf16[1,128]{1,0:T(2,128)(2,1)S(1)}, u32[]{:S(2)}, u32[]{:S(2)}) collective-permute-start(bf16[1,128]{1,0:T(2,128)(2,1)S(1)} %get-tuple-element.13), channel_id=1, source_target_pairs={{0,8},{8,16},{16,24},{24,32},{32,40},{40,48},{48,56},{56,64},{64,7... | collective-permute-start | bytes 776 | tf_op jit(solution)/shard_map/ppermute | solution.py:20
  193.1 4.7 %collective-permute-start.1 = (bf16[1,128]{1,0:T(2,128)(2,1)S(1)}, bf16[1,128]{1,0:T(2,128)(2,1)S(1)}, u32[]{:S(2)}, u32[]{:S(2)}) collective-permute-start(bf16[1,128]{1,0:T(2,128)(2,1)S(1)} %get-tuple-element.14), channel_id=1, source_target_pairs={{8,0},{16,8},{24,16},{32,24},{40,32},{48,40},{56,48},{64,56},{72,6... | collective-permute-start | bytes 776 | tf_op jit(solution)/shard_map/ppermute | solution.py:21
Sparse Core Ops, SparseCore 0:
  13.6 143.5 all-gather.2
  163.2 140.6 all-gather.4
where the time goes:
time: 369 us; the launch traced here: 368 us
  waiting for transfers between devices  240 us (65%)
  blocking collectives  40.1 us (11%)
  matrix products  25.8 us (7%)
  starting transfers between devices  23.1 us (6%)
  local copies, waits for them, and re-layouts  18.1 us (5%)
  between operations  13.7 us (4%)
  other arithmetic  7.19 us (2%)
    all_gather x1, waiting for transfers between devices, turned_gather(): lax.all_gather(both, axis, axis=0, tiled=True)  101 us
    all_gather x1, waiting for transfers between devices, in_one_piece(): lax.all_gather(both, axis, axis=dim, tiled=True)  101 us
    all_to_all x1, blocking collectives, sum_at_owner(): lax.all_to_all(parts, axis, split_axis=0, concat_axis=0, tiled=True)  40.1 us
    all_to_all x2, waiting for transfers between devices, from_everyone(): return lax.all_to_all(copies, axis, split_axis=0, concat_axis=0, tiled=True)  36.4 us
    all_to_all x2, starting transfers between devices, from_everyone(): return lax.all_to_all(copies, axis, split_axis=0, concat_axis=0, tiled=True)  19.5 us
    unnamed x25, local copies, waits for them, and re-layouts  8.42 us
    dot_general x5, matrix products, local(): jnp.dot(normed, weight, preferred_element_type=jnp.float32)  8.2 us
  transfers between devices with their start and end apart: 6, of which 5 were waited for; matrix products, arithmetic and copies ran while one was open for 6% of the time, Pallas kernels for 0%

commit v1 on v0

--- a/solution.py
+++ b/solution.py
@@ -1,7 +1,194 @@
+import functools
 import jax
 import jax.numpy as jnp
 from jax import lax
 from jax.sharding import PartitionSpec as P
+from jax.experimental import pallas as pl
+from jax.experimental.pallas import tpu as pltpu
+
+NZ, NY, NX = 16, 4, 4
+MESH = pl.DeviceIdType.MESH
+BROWS, AROWS = 96, 192
+BF = jnp.bfloat16
+F32 = jnp.float32
+
+
+def place():
+    s, t = lax.axis_index("sp"), lax.axis_index("tp")
+    z, y = s // NY, lax.rem(s, NY)
+    x, c = t // 2, lax.rem(t, 2)
+    return s, t, z, y, x, c
+
+
+def ring(value, step, size):
+    return lax.rem(value + (step + size), size)
+
+
+def gather_kernel(tok, w, X, WA, WB, loc, zas, zar, zbs, zbr, yas, yar, ybs, ybr, xs, xr):
+    s, t, z, y, x, c = place()
+
+    def at(dz=0, dy=0, dx=0, dc=0):
+        return (ring(z, dz, NZ) * NY + ring(y, dy, NY), ring(x, dx, NX) * 2 + ring(c, dc, 2))
+
+    own = [
+        pltpu.make_async_copy(w.at[pl.ds(BROWS, AROWS)], WA.at[z, y], loc.at[0]),
+        pltpu.make_async_copy(w.at[pl.ds(0, BROWS)], WB.at[z, y], loc.at[1]),
+        pltpu.make_async_copy(tok.at[:, pl.ds(0, 128)], X.at[2 * t], loc.at[2]),
+        pltpu.make_async_copy(tok.at[:, pl.ds(128, 128)], X.at[2 * t + 1], loc.at[3]),
+    ]
+    for o in own:
+        o.start()
+    barrier = pltpu.get_barrier_semaphore()
+    near = [at(dz=1), at(dz=-1), at(dy=1), at(dy=-1), at(dx=1), at(dx=-1), at(dc=1)]
+    for d in near:
+        pl.semaphore_signal(barrier, inc=1, device_id=d, device_id_type=MESH)
+    for o in own:
+        o.wait()
+    pl.semaphore_wait(barrier, len(near))
+
+    sent = []
+
+    def push(ref, ssem, rsem, dev):
+        cp = pltpu.make_async_remote_copy(src_ref=ref, dst_ref=ref, send_sem=ssem, recv_sem=rsem, device_id=dev, device_id_type=MESH)
+        cp.start()
+        sent.append(cp)
+
+    def took(ref, ssem, rsem):
+        pltpu.make_async_remote_copy(src_ref=ref, dst_ref=ref, send_sem=ssem, recv_sem=rsem, device_id=at(dz=1), device_id_type=MESH).wait_recv()
+
+    DZ = (1, -1)
+
+    def za(k, d):
+        return (pl.ds(0, AROWS) if k < 8 else pl.ds(d * (AROWS // 2), AROWS // 2))
+
+    def zb(k, d):
+        return (pl.ds(0, BROWS) if k < 8 else pl.ds(d * (BROWS // 2), BROWS // 2))
+
+    def send_za(k):
+        for d in (0, 1):
+            o = ring(z, -DZ[d] * (k - 1), NZ)
+            push(WA.at[o, y, za(k, d)], zas.at[d, k - 1], zar.at[d, k - 1], at(dz=DZ[d]))
+
+    def recv_za(k):
+        for d in (0, 1):
+            o = ring(z, -DZ[d] * k, NZ)
+            took(WA.at[o, y, za(k, d)], zas.at[d, k - 1], zar.at[d, k - 1])
+
+    def send_zb(k, j):
+        for d in (0, 1):
+            o = ring(z, -DZ[d] * (k - 1), NZ)
+            push(WB.at[o, ring(y, j, NY), zb(k, d)], zbs.at[d, k - 1, j], zbr.at[d, k - 1, j], at(dz=DZ[d]))
+
+    def recv_zb(k, j):
+        for d in (0, 1):
+            o = ring(z, -DZ[d] * k, NZ)
+            took(WB.at[o, ring(y, j, NY), zb(k, d)], zbs.at[d, k - 1, j], zbr.at[d, k - 1, j])
+
+    def y_direct(buf, o, ss, rr):
+        for d in (0, 1):
+            push(buf.at[o, y], ss(d), rr(d), at(dy=DZ[d]))
+
+    def y_onward(buf, o, ss, rr, rows):
+        for d in (0, 1):
+            src = ring(y, -DZ[d], NY)
+            took(buf.at[o, src], ss(d), rr(d))
+            push(buf.at[o, src, pl.ds(d * (rows // 2), rows // 2)], ss(2 + d), rr(2 + d), at(dy=DZ[d]))
+
+    def y_last(buf, o, ss, rr, rows):
+        for d in (0, 1):
+            src = ring(y, -2 * DZ[d], NY)
+            took(buf.at[o, src, pl.ds(d * (rows // 2), rows // 2)], ss(2 + d), rr(2 + d))
+
+    def sem2(ref, i):
+        return lambda d: ref.at[d, i]
+
+    def ya(i):
+        return sem2(yas, i), sem2(yar, i)
+
+    def origins(k):
+        if k == 0:
+            return [(0, z)]
+        if k == 8:
+            return [(15, ring(z, 8, NZ))]
+        return [(k, ring(z, -k, NZ)), (7 + k, ring(z, k, NZ))]
+
+    def xblk(tt, half=None):
+        base = 2 * tt
+        return X.at[pl.ds(base, 2)] if half is None else X.at[base + half]
+
+    def same(dx):
+        return ring(x, dx, NX) * 2 + c
+
+    for d in (0, 1):
+        push(xblk(t), xs.at[d], xr.at[d], at(dx=DZ[d]))
+    ybf = lambda d: ybs.at[d]
+    ybg = lambda d: ybr.at[d]
+    y_direct(WB, z, ybf, ybg)
+    send_zb(1, 0)
+    send_za(1)
+    y_direct(WA, z, *ya(0))
+    push(xblk(t), xs.at[4], xr.at[4], at(dc=1))
+    y_onward(WB, z, ybf, ybg, BROWS)
+    send_zb(1, 1)
+    send_zb(1, 3)
+    y_last(WB, z, ybf, ybg, BROWS)
+    send_zb(1, 2)
+    for k in range(1, 9):
+        recv_za(k)
+        if k < 8:
+            send_za(k + 1)
+        for i, o in origins(k):
+            y_direct(WA, o, *ya(i))
+        for j in (0, 1, 3, 2):
+            recv_zb(k, j)
+            if k < 8:
+                send_zb(k + 1, j)
+        for i, o in origins(k - 1):
+            y_onward(WA, o, *ya(i), AROWS)
+        if k == 2:
+            for d in (0, 1):
+                took(xblk(same(-DZ[d])), xs.at[d], xr.at[d])
+                push(xblk(same(-DZ[d]), d), xs.at[2 + d], xr.at[2 + d], at(dx=DZ[d]))
+                push(xblk(same(-DZ[d])), xs.at[5 + d], xr.at[5 + d], at(dc=1))
+        if k == 4:
+            for d in (0, 1):
+                took(xblk(same(-2 * DZ[d]), d), xs.at[2 + d], xr.at[2 + d])
+            push(xblk(same(2)), xs.at[7], xr.at[7], at(dc=1))
+        if k == 5:
+            took(xblk(ring(t, 0, 8) + 1 - 2 * c), xs.at[4], xr.at[4])
+            for d in (0, 1):
+                took(xblk(ring(x, -DZ[d], NX) * 2 + 1 - c), xs.at[5 + d], xr.at[5 + d])
+            took(xblk(ring(x, 2, NX) * 2 + 1 - c), xs.at[7], xr.at[7])
+    for i, o in origins(8):
+        y_onward(WA, o, *ya(i), AROWS)
+    for i in range(16):
+        pass
+    for k in range(0, 9):
+        for i, o in origins(k):
+            y_last(WA, o, *ya(i), AROWS)
+    for cp in sent:
+        cp.wait_send()
+
+
+def gather(tok, w):
+    D = pltpu.SemaphoreType.DMA
+    vm = pl.BlockSpec(memory_space=pltpu.VMEM)
+    anys = pl.BlockSpec(memory_space=pl.ANY)
+    return pl.pallas_call(
+        gather_kernel,
+        out_shape=[
+            jax.ShapeDtypeStruct((16, 512, 128), BF),
+            jax.ShapeDtypeStruct((NZ, NY, AROWS, 128), BF),
+            jax.ShapeDtypeStruct((NZ, NY, BROWS, 128), BF),
+        ],
+        in_specs=[anys, anys],
+        out_specs=[vm] * 3,
+        scratch_shapes=[
+            D((4,)), D((2, 8)), D((2, 8)), D((2, 8, 4)), D((2, 8, 4)),
+            D((4, 16)), D((4, 16)), D((4,)), D((4,)), D((8,)), D((8,)),
+        ],
+        compiler_params=pltpu.CompilerParams(collective_id=0, has_side_effects=True, vmem_limit_bytes=48 * 1024 * 1024),
+    )(tok, w)
 
 HEAD_DIM = 64
 
@@ -206,28 +393,19 @@
     conv_output,
     retention_output,
 ):
-    whole = collect(tokens, "tp", 1)
+    order = (key_proj, value_proj, query_proj, out_gate, inner_gate, conv_input, outer_gate, conv_output.T, retention_output.T)
+    blocks, wa, wb = gather(tokens, jnp.concatenate(order, axis=0))
+    whole = jnp.moveaxis(blocks, 0, 1).reshape(512, 2048)
+    wa = wa.reshape(64, 6, 32, 128)
+    wb = wb.reshape(64, 3, 32, 128)
+    pick = lambda a, i: a[:, i].reshape(2048, 128)
     wide = whole.astype(jnp.float32)
     normed = (
         wide * lax.rsqrt(jnp.mean(wide * wide, axis=-1, keepdims=True) + EPS) * norm_gain
     ).astype(jnp.bfloat16)
     row_count = normed.shape[0]
     offsets = lax.axis_index("sp") * row_count + lax.iota(jnp.int32, row_count)
-    gathered = turned_gather(
-        (
-            outer_gate,
-            inner_gate,
-            conv_input,
-            query_proj,
-            key_proj,
-            value_proj,
-            out_gate,
-            conv_output,
-            retention_output,
-        ),
-        "sp",
-        (0, 0, 0, 0, 0, 0, 0, 1, 1),
-    )
+    gathered = [pick(wa, 3), pick(wa, 1), pick(wa, 2), pick(wb, 2), pick(wb, 0), pick(wb, 1), pick(wa, 0), pick(wa, 4).T, pick(wa, 5).T]
     projected = [
         jnp.dot(normed, weight, preferred_element_type=jnp.float32).astype(jnp.bfloat16)
         for weight in gathered[:7]

time: 369 us -> 287 us (0.78)
  waiting for transfers between devices: 240 us -> 104 us
  Pallas kernels: 0 us -> 52.5 us
  starting transfers between devices: 23.1 us -> 14.8 us
  local copies, waits for them, and re-layouts: 18.1 us -> 25.6 us
  other arithmetic: 7.19 us -> 11.1 us
    all_gather x1 -> x0, waiting for transfers between devices: 101 us -> none  [turned_gather(): lax.all_gather(both, axis, axis=0, tiled=True)]
    pallas_call x0 -> x1, Pallas kernels: none -> 52.5 us  [gather(): pl.pallas_call(gather_kernel, out_shape=[jax.ShapeDtypeStruct((16, 512, 1...]
    all_to_all x2 -> x1, waiting for transfers between devices: 36.4 us -> 0.01 us  [from_everyone(): return lax.all_to_all(copies, axis, split_axis=0, concat_axis=0, tiled=True)]
    all_to_all x2 -> x1, starting transfers between devices: 19.5 us -> 10.4 us  [from_everyone(): return lax.all_to_all(copies, axis, split_axis=0, concat_axis=0, tiled=True)]
    slice x1 -> x3, local copies, waits for them, and re-layouts: 0.16 us -> 4.77 us  [the longest x2 4.61 us: local(): pick = lambda a, i: a[:, i].reshape(2048, 128)]
    dot_general x5, matrix products: 8.2 us -> 4.04 us  [local(): jnp.dot(normed, weight, preferred_element_type=jnp.float32)]
    unnamed x25 -> x46, local copies, waits for them, and re-layouts: 8.42 us -> 7.79 us
  transfers between devices with their start and end apart: 6 -> 4, of which waited for: 5 -> 1; matrix products, arithmetic and copies ran while one was open for 6% -> 7% of each run, Pallas kernels for 0% -> 0%
where the time goes in v1:
time: 287 us; the launch traced here: 286 us
  waiting for transfers between devices  104 us (36%)
  Pallas kernels  52.5 us (18%)
  blocking collectives  40.1 us (14%)
  local copies, waits for them, and re-layouts  25.6 us (9%)
  matrix products  24 us (8%)
  starting transfers between devices  14.8 us (5%)
  between operations  13.7 us (5%)
  other arithmetic  11.1 us (4%)
    all_gather x1, waiting for transfers between devices, in_one_piece(): lax.all_gather(both, axis, axis=dim, tiled=True)  104 us
    pallas_call x1, Pallas kernels, gather(): pl.pallas_call(gather_kernel, out_shape=[jax.ShapeDtypeStruct((16, 512, 1...  52.5 us
    all_to_all x1, blocking collectives, sum_at_owner(): lax.all_to_all(parts, axis, split_axis=0, concat_axis=0, tiled=True)  40.1 us
    all_to_all x1, starting transfers between devices, from_everyone(): return lax.all_to_all(copies, axis, split_axis=0, concat_axis=0, tiled=True)  10.4 us
    unnamed x46, local copies, waits for them, and re-layouts  7.79 us
    dot_general x1, matrix products, local(): jnp.dot(ret_out, ret_weight, preferred_element_type=jnp.float32)  5.87 us
  transfers between devices with their start and end apart: 4, of which 1 were waited for; matrix products, arithmetic and copies ran while one was open for 7% of the time, Pallas kernels for 0%

profile of v1, /device:TPU:1, one launch (start us, length us, event | category | flops | bytes accessed | tf_op | source)
XLA Modules:
  0.0 286.1 jit_solution(12431888245512967448)
XLA Ops:
  16.8 0.9 copy-done
  17.8 52.5 %shard_map.136 = (bf16[16,512,128]{2,1,0:T(8,128)(2,1)S(1)}, bf16[16,4,192,128]{3,2,1,0:T(8,128)(2,1)}, bf16[16,4,96,128]{3,2,1,0:T(8,128)(2,1)S(1)}) custom-call(bf16[512,256]{1,0:T(8,128)(2,1)S(1)} %copy-done, bf16[288,128]{1,0:T(8,128)(2,1)S(1)} %constant_dynamic-update-slice_fusion.w), custom_call_target="tpu_custom_call" | custom-call | tf_op jit(solution)/shard_map/pallas_call | solution.py:177
  70.3 1.1 fusion.62
  71.9 2.1 fusion.7
  74.0 2.9 copy.26
  76.9 1.5 convolution_convert_fusion
  82.2 10.4 %all-to-all-start = ((f32[64,1,2,2]{3,2,1,0:T(2,128)}), f32[64,1,2,2]{3,2,1,0:T(2,128)S(1)}, u32[]{:S(2)}, u32[]{:S(2)}) async-start(f32[64,1,2,2]{3,2,1,0:T(2,128)} %broadcast_in_dim.32), calls=%async_computation | async-start | bytes 131072 | tf_op jit(solution)/shard_map/all_to_all | solution.py:215
  92.5 3.5 %fusion.61 = (bf16[64,1,32,128]{3,2,1,0:T(8,128)(2,1)S(1)}, bf16[64,1,32,128]{3,2,1,0:T(8,128)(2,1)S(1)}, bf16[64,1,32,128]{3,2,1,0:T(8,128)(2,1)}, bf16[64,1,32...) fusion(bf16[64,6,32,128]{3,2,1,0:T(8,128)(2,1)} %bitcast.150), kind=kLoop, calls=%fused_computation.125 | loop fusion | bytes 6291456 | tf_op jit(solution)/shard_map/slice | solution.py:401
  97.6 2.9 %collective-permute-start = (bf16[1,128]{1,0:T(2,128)(2,1)S(1)}, bf16[1,128]{1,0:T(2,128)(2,1)S(1)}, u32[]{:S(2)}, u32[]{:S(2)}) collective-permute-start(bf16[1,128]{1,0:T(2,128)(2,1)S(1)} %get-tuple-element.28), channel_id=1, source_target_pairs={{0,8},{8,16},{16,24},{24,32},{32,40},{40,48},{48,56},{56,64},{64,7... | collective-permute-start | bytes 776 | tf_op jit(solution)/shard_map/ppermute | solution.py:207
  100.5 1.5 collective-permute-start.1
  102.6 0.8 iota_compare_fusion
  103.9 2.9 %fusion.13 = f32[512,2,64]{0,2,1:T(8,128)} fusion(bf16[512,2,64]{0,2,1:T(8,128)(2,1)} %bitcast.178, f32[2,512]{1,0:T(2,128)S(1)} %rev.8, f32[2,512]{1,0:T(2,128)S(1)} %bitcast.167, pred[512,512]{1,0:T(8,128)(4,1)} %iota_compare_fusion, bf16[512,2,32]{0,2,1:T(8,128)(2,1)S(1)} %get-tuple-element.26, bf16[512,2,32]{0,2,1:T(8,128)(2,1)S(1)} %get-tuple-element.27, ...), kind=kOutput, calls=%fused_computation.19 | convolution fusion | flops 137297920 | bytes 1056768 | tf_op jit(solution)/shard_map/hij,jhe->ihe/dot_general | solution.py:298
  107.4 0.9 maximum_convert_fusion
  108.4 5.5 %fusion.22 = f32[512,2048]{1,0:T(8,128)} fusion(bf16[2048,128]{1,0:T(8,128)(2,1)} %bitcast.153, bf16[512,2048]{0,1:T(8,128)(2,1)S(1)} %bitcast.147, bf16[2048,128]{1,0:T(8,128)(2,1)} %bitcast.154, f32[514,128]{1,0:T(8,128)S(1)} %maximum_convert_fusion, f32[128]{0:T(128)} %get-tuple-element.39, f32[128]{0:T(128)} %get-tuple-element.40, f32[128]{0:T(128)} %get-tuple-element.38), kind=kOutput, calls=%fused_computation.35 | convolution fusion | flops 537460736 | bytes 8128000 | tf_op jit(solution)/shard_map/dot_general | solution.py:421
  115.6 104.2 %all-gather.2.cloned.1.call-done = bf16[64,4,64,64]{3,2,1,0:T(8,128)(2,1)} async-done(((bf16[1,4,64,64]{3,2,1,0:T(8,128)(2,1)}), bf16[64,4,64,64]{3,2,1,0:T(8,128)(2,1)}) %all-gather.2.cloned.1.call-update) | async-done | bytes 2097168 | tf_op jit(solution)/shard_map/all_gather | solution.py:235
  219.8 5.0 %fusion.60 = (bf16[64,2,64,64]{3,2,1,0:T(8,128)(2,1)S(1)}, bf16[64,2,64,64]{3,2,1,0:T(8,128)(2,1)}) fusion(bf16[64,4,64,64]{3,2,1,0:T(8,128)(2,1)} %all-gather.2.cloned.1.call-done), kind=kLoop, calls=%fused_computation.124 | loop fusion | bytes 4194304 | tf_op jit(solution)/shard_map/split | solution.py:235
  224.7 1.2 fusion.3
  226.1 2.8 fusion.5
  229.0 1.1 fusion.12
  230.3 0.8 multiply_multiply_fusion
  231.1 1.1 copy.31
  232.2 5.9 %add_convert_fusion = bf16[512,2048]{1,0:T(8,128)(2,1)} fusion(f32[512,2048]{1,0:T(8,128)} %fusion.22, bf16[2048,128]{1,0:T(8,128)(2,1)S(1)} %bitcast.152, f32[512,128]{1,0:T(8,128)S(1)} %copy.31, bf16[512,2048]{0,1:T(8,128)(2,1)S(1)} %bitcast.148, bf16[2048,128]{1,0:T(8,128)(2,1)S(1)} %bitcast.151), kind=kOutput, calls=%fused_computation.9 | convolution fusion | flops 539492352 | bytes 9699328 | tf_op jit(solution)/shard_map/dot_general | solution.py:422
  238.1 40.1 %all_to_all.10 = bf16[8,64,2048]{2,1,0:T(8,128)(2,1)S(1)} all-to-all(bf16[8,64,2048]{2,1,0:T(8,128)(2,1)} %bitcast.149), channel_id=1, replica_groups=mesh['sp'=64,'tp'=8] {'tp'}, dimensions={0} | all-to-all | bytes 4194304 | tf_op jit(solution)/shard_map/all_to_all | solution.py:256
  278.2 1.1 reduce_sum.32
  (103 shorter events, 19.7 us)
Async XLA Ops:
  6.5 213.2 %all-gather.2.cloned.1.call-start = ((), (), s32[]{:S(2)}) async-start(), calls=%async_computation.2 | async-start | bytes 4259840 | tf_op jit(solution)/shard_map/all_gather | solution.py:235
  10.2 61.3 %copy-start.7 = (f32[1,2,4,128]{3,1,2,0:T(2,128)}, f32[1,2,4,128]{3,1,2,0:T(2,128)S(1)}, u32[]{:S(2)}) copy-start(f32[1,2,4,128]{3,1,2,0:T(2,128)S(1)} %copy.53) | copy-start | bytes 12292
  10.3 61.1 %copy-start.9 = (f32[2,1]{0,1:T(1,128)}, f32[2,1]{0,1:T(1,128)S(1)}, u32[]{:S(2)}) copy-start(f32[2,1]{0,1:T(1,128)S(1)} %copy.38) | copy-start | bytes 28
  10.4 69.1 %copy-start.11 = (f32[2,1]{0,1:T(1,128)}, f32[2,1]{0,1:T(1,128)S(1)}, u32[]{:S(2)}) copy-start(f32[2,1]{0,1:T(1,128)S(1)} %copy.39) | copy-start | bytes 28
  16.8 0.9 copy-start
  70.3 1.6 copy-start.6
  79.4 13.1 %copy-start.16 = (bf16[512,128]{0,1:T(8,128)(2,1)}, bf16[512,128]{0,1:T(8,128)(2,1)S(1)}, u32[]{:S(2)}) copy-start(bf16[512,128]{0,1:T(8,128)(2,1)S(1)} %convolution_convert_fusion.2) | copy-start | bytes 393220
  79.4 2.0 copy-start.10
  79.6 1.9 copy-start.12
  80.0 0.7 copy-start.5
  80.0 2.2 copy-start.4
  80.0 23.9 %copy-start.1 = (bf16[512,2,32]{0,2,1:T(8,128)(2,1)}, bf16[512,2,32]{0,2,1:T(8,128)(2,1)S(1)}, u32[]{:S(2)}) copy-start(bf16[512,2,32]{0,2,1:T(8,128)(2,1)S(1)} %get-tuple-element.27) | copy-start | bytes 196612
  82.2 31.8 %all-to-all-start = ((f32[64,1,2,2]{3,2,1,0:T(2,128)}), f32[64,1,2,2]{3,2,1,0:T(2,128)S(1)}, u32[]{:S(2)}, u32[]{:S(2)}) async-start(f32[64,1,2,2]{3,2,1,0:T(2,128)} %broadcast_in_dim.32), calls=%async_computation | async-start | bytes 131072 | tf_op jit(solution)/shard_map/all_to_all | solution.py:215
  96.8 6.5 %copy-start.13 = (f32[3,128]{1,0:T(4,128)S(1)}, f32[3,128]{1,0:T(4,128)}, u32[]{:S(2)}) copy-start(f32[3,128]{1,0:T(4,128)} %param.23) | copy-start | bytes 4612
  96.8 7.1 %copy-start.8 = (f32[1,2,4,128]{3,1,2,0:T(2,128)S(1)}, f32[1,2,4,128]{3,1,2,0:T(2,128)}, u32[]{:S(2)}) copy-start(f32[1,2,4,128]{3,1,2,0:T(2,128)} %copy-done.7) | copy-start | bytes 12292
  97.6 9.3 %copy-start.3 = (bf16[512,128]{1,0:T(8,128)(2,1)}, bf16[512,128]{1,0:T(8,128)(2,1)S(1)}, u32[]{:S(2)}) copy-start(bf16[512,128]{1,0:T(8,128)(2,1)S(1)} %fusion.17) | copy-start | bytes 393220
  97.6 9.3 %collective-permute-start = (bf16[1,128]{1,0:T(2,128)(2,1)S(1)}, bf16[1,128]{1,0:T(2,128)(2,1)S(1)}, u32[]{:S(2)}, u32[]{:S(2)}) collective-permute-start(bf16[1,128]{1,0:T(2,128)(2,1)S(1)} %get-tuple-element.28), channel_id=1, source_target_pairs={{0,8},{8,16},{16,24},{24,32},{32,40},{40,48},{48,56},{56,64},{64,7... | collective-permute-start | bytes 776 | tf_op jit(solution)/shard_map/ppermute | solution.py:207
  100.5 6.9 %collective-permute-start.1 = (bf16[1,128]{1,0:T(2,128)(2,1)S(1)}, bf16[1,128]{1,0:T(2,128)(2,1)}, u32[]{:S(2)}, u32[]{:S(2)}) collective-permute-start(bf16[1,128]{1,0:T(2,128)(2,1)S(1)} %get-tuple-element.29), channel_id=1, source_target_pairs={{8,0},{16,8},{24,16},{32,24},{40,32},{48,40},{56,48},{64,56},{72,6... | collective-permute-start | bytes 776 | tf_op jit(solution)/shard_map/ppermute | solution.py:208
  103.9 2.9 %copy-start.15 = (f32[128]{0:T(128)S(1)}, f32[128]{0:T(128)}, u32[]{:S(2)}) copy-start(f32[128]{0:T(128)} %param.25) | copy-start | bytes 1540
  106.9 0.5 copy-start.14
  224.7 4.3 %copy-start.2 = (bf16[512,2,32]{0,2,1:T(8,128)(2,1)S(1)}, bf16[512,2,32]{0,2,1:T(8,128)(2,1)}, u32[]{:S(2)}) copy-start(bf16[512,2,32]{0,2,1:T(8,128)(2,1)} %copy-done.1) | copy-start | bytes 196612
Sparse Core Ops, SparseCore 0:
  81.6 138.1 all-gather.1

commit v2 on v1

v2 whole, which is shorter than its diff:
```python
import math

import jax
import jax.numpy as jnp
from jax import lax
from jax.experimental import pallas as pl
from jax.experimental.pallas import tpu as pltpu
from jax.sharding import PartitionSpec as P

NZ, NY, NX = 16, 4, 4
SPAN, HEAD = 512, 64
EPS, THETA = 1e-06, 10000.0
BROWS, AROWS = 96, 192
MESH = pl.DeviceIdType.MESH
BF, F32 = jnp.bfloat16, jnp.float32
EXACT = lax.Precision.HIGHEST
SIDES = (1, -1)


def ring(value, step, size):
    return lax.rem(value + (step + size), size)


def rows_of(i, n):
    return pl.ds(pl.multiple_of(i * n, n), n)


def nn(a, b, precision=None):
    return lax.dot_general(a, b, (((1,), (0,)), ((), ())), precision=precision, preferred_element_type=F32)


def nt(a, b, precision=None):
    return lax.dot_general(a, b, (((1,), (1,)), ((), ())), precision=precision, preferred_element_type=F32)


def tn(a, b):
    return lax.dot_general(a, b, (((0,), (0,)), ((), ())), preferred_element_type=F32)


def left_head(shape):
    return lax.broadcasted_iota(jnp.int32, shape, len(shape) - 1) < HEAD


def mixer_kernel(
    tok, gain, outer_w, inner_w, conv_w, query_w, key_w, value_w, gate_w, taps, decay, head_gain, conv_o, ret_o,
    out,
    X, NR, WA, WB, WO, accb, acca, D, scale, trig, qkv, mix, CR, halo_s, halo_r,
    msg_a, got_a, msg_b, got_b, msg_c, got_c, part, pair, quads, via, fin,
    loc, zas, zar, zbs, zbr, yas, yar, ybs, ybr, xs, xr, hs, hr, sas, sar, sbs, sbr, scs, scr, ds, dr, vs, vr, fs, fr,
):
    s, t = lax.axis_index("sp"), lax.axis_index("tp")
    z, y, x, c = s // NY, lax.rem(s, NY), t // 2, lax.rem(t, 2)

    def at(dz=0, dy=0, dx=0, dc=0):
        return (ring(z, dz, NZ) * NY + ring(y, dy, NY), ring(x, dx, NX) * 2 + ring(c, dc, 2))

    sent = []

    def push(src, dst, ssem, rsem, dev):
        cp = pltpu.make_async_remote_copy(
            src_ref=src, dst_ref=dst, send_sem=ssem, recv_sem=rsem, device_id=dev, device_id_type=MESH
        )
        cp.start()
        sent.append(cp)

    def took(ref, ssem, rsem):
        pltpu.make_async_remote_copy(
            src_ref=ref, dst_ref=ref, send_sem=ssem, recv_sem=rsem, device_id=at(dz=1), device_id_type=MESH
        ).wait_recv()

    own = [
        pltpu.make_async_copy(tok.at[:, pl.ds(0, 128)], X.at[2 * t], loc.at[0]),
        pltpu.make_async_copy(tok.at[:, pl.ds(128, 128)], X.at[2 * t + 1], loc.at[1]),
    ]
    for i, w in enumerate((key_w, value_w, query_w)):
        own.append(pltpu.make_async_copy(w, WB.at[z, y, pl.ds(32 * i, 32)], loc.at[2 + i]))
    for i, w in enumerate((gate_w, inner_w, conv_w, outer_w)):
        own.append(pltpu.make_async_copy(w, WA.at[z, y, pl.ds(32 * i, 32)], loc.at[5 + i]))
    for o in own:
        o.start()
    WA[z, y, pl.ds(128, 32)] = conv_o[...]
    WA[z, y, pl.ds(160, 32)] = ret_o[...]
    barrier = pltpu.get_barrier_semaphore()
    near = [at(dz=1), at(dz=-1), at(dy=1), at(dy=-1), at(dx=1), at(dx=-1), at(dc=1)]
    for d in near:
        pl.semaphore_signal(barrier, inc=1, device_id=d, device_id_type=MESH)
    for o in own:
        o.wait()
    pl.semaphore_wait(barrier, len(near))

    def half_or_all(k, d, rows):
        return pl.ds(0, rows) if k < 8 else pl.ds(d * (rows // 2), rows // 2)

    def send_za(k):
        for d in (0, 1):
            ref = WA.at[ring(z, -SIDES[d] * (k - 1), NZ), y, half_or_all(k, d, AROWS)]
            push(ref, ref, zas.at[d, k - 1], zar.at[d, k - 1], at(dz=SIDES[d]))

    def recv_za(k):
        for d in (0, 1):
            took(WA.at[ring(z, -SIDES[d] * k, NZ), y, half_or_all(k, d, AROWS)], zas.at[d, k - 1], zar.at[d, k - 1])

    def send_zb(k, j):
        for d in (0, 1):
            ref = WB.at[ring(z, -SIDES[d] * (k - 1), NZ), ring(y, j, NY), half_or_all(k, d, BROWS)]
            push(ref, ref, zbs.at[d, k - 1, j], zbr.at[d, k - 1, j], at(dz=SIDES[d]))

    def recv_zb(k, j):
        for d in (0, 1):
            ref = WB.at[ring(z, -SIDES[d] * k, NZ), ring(y, j, NY), half_or_all(k, d, BROWS)]
            took(ref, zbs.at[d, k - 1, j], zbr.at[d, k - 1, j])

    def y_direct(buf, o, ss, rr):
        for d in (0, 1):
            push(buf.at[o, y], buf.at[o, y], ss(d), rr(d), at(dy=SIDES[d]))

    def y_onward(buf, o, ss, rr, rows):
        for d in (0, 1):
            src = ring(y, -SIDES[d], NY)
            took(buf.at[o, src], ss(d), rr(d))
            ref = buf.at[o, src, pl.ds(d * (rows // 2), rows // 2)]
            push(ref, ref, ss(2 + d), rr(2 + d), at(dy=SIDES[d]))

    def y_last(buf, o, ss, rr, rows):
        for d in (0, 1):
            src = ring(y, -2 * SIDES[d], NY)
            took(buf.at[o, src, pl.ds(d * (rows // 2), rows // 2)], ss(2 + d), rr(2 + d))

    def ya(i):
        return (lambda d: yas.at[d, i]), (lambda d: yar.at[d, i])

    def origins(k):
        if k == 0:
            return [(0, z)]
        if k == 8:
            return [(15, ring(z, 8, NZ))]
        return [(k, ring(z, -k, NZ)), (7 + k, ring(z, k, NZ))]

    yb = (lambda d: ybs.at[d]), (lambda d: ybr.at[d])

    def xblk(tt, half=None):
        return X.at[pl.ds(2 * tt, 2)] if half is None else X.at[2 * tt + half]

    def on_x(dx, core):
        return ring(x, dx, NX) * 2 + core

    def xpush(tt, half, i, dev):
        push(xblk(tt, half), xblk(tt, half), xs.at[i], xr.at[i], dev)

    def decay_sums():
        row = lax.broadcasted_iota(jnp.int32, (SPAN, SPAN), 0)
        col = lax.broadcasted_iota(jnp.int32, (SPAN, SPAN), 1)
        lower = (col <= row).astype(F32)
        upper = (col >= row).astype(F32)
        for i, tri in enumerate((lower, upper)):
            rates = decay[i]
            along = jnp.concatenate([rates, jnp.zeros((6, SPAN), F32)], axis=0)
            over = nt(along, tri, EXACT)
            mix[pl.ds(i * 8, 8), :] = over
            columns = [nt(tri, jnp.broadcast_to(rates[h : h + 1], (128, SPAN)), EXACT) for h in (0, 1)]
            for h in (0, 1):
                scale[2 * i + h] = columns[h]

    def decay_matrix(h):
        row = lax.broadcasted_iota(jnp.int32, (128, SPAN), 0)
        col = lax.broadcasted_iota(jnp.int32, (128, SPAN), 1)

        def chunk(i, _):
            wide = lambda a: jnp.concatenate([a] * 4, axis=1)
            cf = wide(scale[h, rows_of(i, 128)]) - mix[pl.ds(h, 1), :]
            rb = wide(scale[2 + h, rows_of(i, 128)]) - mix[pl.ds(8 + h, 1), :]
            D[h, rows_of(i, 128)] = jnp.exp(jnp.where(col <= row + i * 128, cf, rb))
            return 0

        lax.fori_loop(0, 4, chunk, 0)

    def decay_scales():
        left = left_head((SPAN, 128))
        cf = jnp.where(left, scale[0], scale[1])
        rb = jnp.where(left, scale[2], scale[3])
        scale[0] = jnp.exp(cf)
        scale[1] = jnp.exp(rb)
        scale[2] = jnp.exp(cf[SPAN - 1 : SPAN] - cf)
        scale[3] = jnp.exp(rb[0:1] - rb)
        tot = jnp.where(lax.broadcasted_iota(jnp.int32, (8, 128), 0) == 0, cf[SPAN - 1 : SPAN], rb[0:1])
        for q in range(NY):
            msg_a[q, pl.ds(32, 8)] = tot

    def angles():
        def chunk(i, _):
            lane = lax.broadcasted_iota(jnp.int32, (128, 128), 1)
            pos = (lax.broadcasted_iota(jnp.int32, (128, 128), 0) + (s * SPAN + i * 128)).astype(F32)
            freq = jnp.exp(-math.log(THETA) * lax.rem(lane, 32).astype(F32) * (2.0 / HEAD))
            ang = pos * freq
            trig[0, rows_of(i, 128)] = jnp.cos(ang)
            sine = jnp.sin(ang)
            trig[1, rows_of(i, 128)] = jnp.where(lax.rem(lane, HEAD) < HEAD // 2, -sine, sine)
            return 0

        lax.fori_loop(0, 4, chunk, 0)

    def normalise():
        def chunk(i, _):
            r = rows_of(i, 64)
            total = jnp.zeros((64, 128), F32)
            for b in range(16):
                w = X[b, r].astype(F32)
                total = total + w * w
            inv = lax.rsqrt(jnp.sum(total, axis=1, keepdims=True) * (1.0 / 2048) + EPS)
            for b in range(16):
                NR[b, r] = (X[b, r].astype(F32) * inv * gain[pl.ds(b, 1), :]).astype(BF)
            return 0

        lax.fori_loop(0, 8, chunk, 0)

    def project(buf, acc, count, k):
        o1, o2 = (ring(z, -k, NZ), ring(z, k, NZ)) if k else (z, ring(z, 8, NZ))
        lhs = jnp.concatenate([NR[o1], NR[o2]], axis=1)
        for i in range(count):
            w = jnp.concatenate([buf[o, :, pl.ds(32 * i, 32), :].reshape(128, 128) for o in (o1, o2)], axis=0)
            part_sum = nn(lhs, w)
            acc[i] = part_sum if k == 1 else acc[i] + part_sum

    def turn_output(k):
        for _, o in origins(k):
            for i in (0, 1):
                w = WA[o, :, pl.ds(128 + 32 * i, 32), :].reshape(128, 128)
                WO[pl.ds(128 * i, 128), pl.ds(pl.multiple_of(o * 128, 128), 128)] = w.T

    def rotated(a):
        wide = a.astype(BF).astype(F32)
        first = lax.rem(lax.broadcasted_iota(jnp.int32, wide.shape, 1), HEAD) < HEAD // 2
        other = jnp.where(first, pltpu.roll(wide, 96, axis=1), pltpu.roll(wide, 32, axis=1))
        return wide * trig[0] + other * trig[1]

    def states():
        rk = (rotated(accb[0]) * HEAD**-0.5).astype(BF)
        value = accb[1].astype(BF)
        qkv[1] = rk
        qkv[2] = value
        wide = rk.astype(F32)
        left = left_head((HEAD, 128))
        for i in (0, 1):
            full = tn((wide * scale[2 + i]).astype(BF), value)
            packed = jnp.where(left, full[0:HEAD], full[HEAD:])
            for q in range(NY):
                msg_a[q, pl.ds(16 * i, 16)] = packed[16 * q : 16 * q + 16]

    def attend():
        qkv[0] = rotated(accb[2]).astype(BF)
        rk, value = qkv[1], qkv[2]

        def chunk(i, _):
            r = rows_of(i, 128)
            rq = qkv[0, r]
            left = left_head((128, 128))
            zero = jnp.zeros_like(rq)
            parts = []
            for h, own_q in enumerate((jnp.where(left, rq, zero), jnp.where(left, zero, rq))):
                probs = (nt(own_q, rk) * D[h, r]).astype(BF)
                parts.append(nn(probs, value))
            mix[r, pl.ds(0, 128)] = jnp.where(left, parts[0], parts[1])
            return 0

        lax.fori_loop(0, 4, chunk, 0)

    def inner_value():
        return (acca[1].astype(BF).astype(F32) * acca[2].astype(BF).astype(F32)).astype(BF).astype(F32)

    def halo_send():
        inner = inner_value()
        halo_s[0] = inner[0:8]
        halo_s[1] = inner[SPAN - 8 :]
        push(halo_s.at[1], halo_r.at[0], hs.at[0], hr.at[0], (lax.rem(s + 1, NZ * NY), t))
        push(halo_s.at[0], halo_r.at[1], hs.at[1], hr.at[1], (lax.rem(s + NZ * NY - 1, NZ * NY), t))

    def convolve():
        for i in (0, 1):
            took(halo_r.at[i], hs.at[i], hr.at[i])
        inner = inner_value()
        row = lax.broadcasted_iota(jnp.int32, (SPAN, 128), 0)
        before = jnp.where(s == 0, 0.0, halo_r[0, 7:8, :])
        after = jnp.where(s == NZ * NY - 1, 0.0, halo_r[1, 0:1, :])
        prev = jnp.where(row == 0, before, pltpu.roll(inner, 1, axis=0))
        follow = jnp.where(row == SPAN - 1, after, pltpu.roll(inner, SPAN - 1, axis=0))
        conv = taps[0:1, :] * prev + taps[1:2, :] * inner + taps[2:3, :] * follow
        CR[:, pl.ds(0, 128)] = (acca[3].astype(BF).astype(F32) * conv).astype(BF)

    def spread_states():
        for dy in (1, 2, 3):
            yy = ring(y, dy, NY)
            push(msg_a.at[yy], got_a.at[y], sas.at[dy - 1], sar.at[dy - 1], at(dy=dy))
        got_a[y] = msg_a[y]

    def step_terms():
        return [
            (got_a[m, pl.ds(0, 16)], got_a[m, pl.ds(16, 16)], jnp.exp(got_a[m, pl.ds(32, 1)]), jnp.exp(got_a[m, pl.ds(33, 1)]))
            for m in range(NY)
        ]

    def spread_rows():
        for dy in (1, 2, 3):
            took(got_a.at[ring(y, -dy, NY)], sas.at[dy - 1], sar.at[dy - 1])
        terms = step_terms()
        fwd, bwd = terms[0][0], terms[NY - 1][1]
        for m in range(1, NY):
            fwd = terms[m][2] * fwd + terms[m][0]
            back = terms[NY - 1 - m]
            bwd = back[3] * bwd + back[1]
        msg_b[0, pl.ds(0, 16)] = fwd
        msg_b[1, pl.ds(0, 16)] = bwd
        for i in (0, 1):
            total = got_a[0, pl.ds(32 + i, 1)]
            for m in range(1, NY):
                total = total + got_a[m, pl.ds(32 + i, 1)]
            msg_b[i, pl.ds(16, 8)] = jnp.broadcast_to(total, (8, 128))
        for d in (8, 7, 9, 6, 10, 5, 11, 4, 12, 3, 13, 2, 14, 1, 15):
            push(msg_b.at[(z + d) // NZ], got_b.at[d], sbs.at[d], sbr.at[d], at(dz=d))

    def return_rows():
        for d in range(1, NZ):
            took(got_b.at[d], sbs.at[d], sbr.at[d])
        fwd = jnp.zeros((16, 128), F32)
        bwd = jnp.zeros((16, 128), F32)
        for d in range(NZ - 1, 0, -1):
            lower = jnp.exp(got_b[d, pl.ds(16, 1)]) * fwd + got_b[d, pl.ds(0, 16)]
            fwd = jnp.where(d <= z, lower, fwd)
            e = NZ - d
            higher = jnp.exp(got_b[e, pl.ds(16, 1)]) * bwd + got_b[e, pl.ds(0, 16)]
            bwd = jnp.where(d <= NZ - 1 - z, higher, bwd)
        terms = step_terms()
        for m in range(NY):
            msg_c[m, pl.ds(0, 16)] = fwd.astype(BF)
            fwd = terms[m][2] * fwd + terms[m][0]
            n = NY - 1 - m
            msg_c[n, pl.ds(16, 16)] = bwd.astype(BF)
            bwd = terms[n][3] * bwd + terms[n][1]
        for dy in (2, 1, 3):
            yy = ring(y, dy, NY)
            push(msg_c.at[yy], got_c.at[y], scs.at[dy - 1], scr.at[dy - 1], at(dy=dy))
        got_c[y] = msg_c[y]

    def finish():
        for dy in (1, 2, 3):
            took(got_c.at[ring(y, -dy, NY)], scs.at[dy - 1], scr.at[dy - 1])
        left = left_head((HEAD, 128))
        into = []
        for i in (0, 1):
            packed = jnp.concatenate([got_c[q, pl.ds(16 * i, 16)] for q in range(NY)], axis=0)
            zero = jnp.zeros_like(packed)
            into.append(jnp.concatenate([jnp.where(left, packed, zero), jnp.where(left, zero, packed)], axis=0))
        both = jnp.concatenate(into, axis=1)
        same = (
            (lax.broadcasted_iota(jnp.int32, (128, 128), 0) < HEAD) == (lax.broadcasted_iota(jnp.int32, (128, 128), 1) < HEAD)
        ).astype(F32) * (1.0 / HEAD)

        def chunk(i, _):
            r = rows_of(i, 128)
            carried = nn(qkv[0, r], both)
            m = mix[r, pl.ds(0, 128)] + scale[0, r] * carried[:, :128] + scale[1, r] * carried[:, 128:]
            inv = lax.rsqrt(nn(m * m, same, EXACT) + EPS)
            g = acca[0, r].astype(BF).astype(F32)
            silu = g / (1.0 + jnp.exp(-g))
            CR[r, pl.ds(128, 128)] = (silu * (m * inv * head_gain[...])).astype(BF)
            return 0

        lax.fori_loop(0, 4, chunk, 0)

    def out_rows(xo):
        rows = CR[rows_of(ring(x, xo, NX), 128)]
        for n in range(4):
            cols = pl.ds(512 * n, 512)
            res = nn(rows, WO[:, cols]).astype(BF).reshape(2, 64, 512)
            part[xo, :, n // 2, :, pl.ds(512 * (n % 2), 512)] = res
        push(part.at[xo, 1 - c], pair.at[xo], ds.at[xo], dr.at[xo], at(dc=1))

    def summed(xo, half):
        return part[xo, c, half].astype(F32) + pair[xo, half].astype(F32)

    def reduce_out():
        for xo in (2, 1, 3, 0):
            out_rows(xo)
        took(pair.at[2], ds.at[2], dr.at[2])
        for h in (0, 1):
            quads[2, h] = summed(2, h).astype(BF)
            push(quads.at[2, h], via.at[h], vs.at[h], vr.at[h], at(dx=SIDES[h]))
        for xo, d in ((1, 0), (3, 1)):
            took(pair.at[xo], ds.at[xo], dr.at[xo])
            quads[xo, 1 - d] = summed(xo, 1 - d).astype(BF)
            push(quads.at[xo, 1 - d], fin.at[d, 1 - d], fs.at[d, 1 - d], fr.at[d, 1 - d], at(dx=SIDES[d]))
        for xo, d in ((1, 0), (3, 1)):
            took(via.at[d], vs.at[d], vr.at[d])
            quads[xo, d] = (summed(xo, d) + via[d].astype(F32)).astype(BF)
            push(quads.at[xo, d], fin.at[d, d], fs.at[d, d], fr.at[d, d], at(dx=SIDES[d]))
        took(pair.at[0], ds.at[0], dr.at[0])
        for h in (0, 1):
            for d in (0, 1):
                took(fin.at[d, h], fs.at[d, h], fr.at[d, h])
            out[:, pl.ds(1024 * h, 1024)] = (summed(0, h) + fin[0, h].astype(F32) + fin[1, h].astype(F32)).astype(BF)

    for d in (0, 1):
        xpush(t, None, d, at(dx=SIDES[d]))
    y_direct(WB, z, *yb)
    send_zb(1, 0)
    send_za(1)
    y_direct(WA, z, *ya(0))
    xpush(t, None, 4, at(dc=1))
    y_onward(WB, z, *yb, BROWS)
    send_zb(1, 1)
    send_zb(1, 3)
    y_last(WB, z, *yb, BROWS)
    send_zb(1, 2)
    decay_sums()
    for k in range(1, 9):
        recv_za(k)
        if k < 8:
            send_za(k + 1)
        for i, o in origins(k):
            y_direct(WA, o, *ya(i))
        for j in (0, 1, 3, 2):
            recv_zb(k, j)
            if k < 8:
                send_zb(k + 1, j)
        for i, o in origins(k - 1):
            y_onward(WA, o, *ya(i), AROWS)
        if k == 1:
            decay_matrix(0)
        if k == 2:
            for d in (0, 1):
                src = on_x(-SIDES[d], c)
                took(xblk(src), xs.at[d], xr.at[d])
                xpush(src, d, 2 + d, at(dx=SIDES[d]))
                xpush(src, None, 5 + d, at(dc=1))
            decay_matrix(1)
        if k == 3:
            decay_scales()
        if k == 4:
            for d in (0, 1):
                took(xblk(on_x(2, c), d), xs.at[2 + d], xr.at[2 + d])
            xpush(on_x(2, c), None, 7, at(dc=1))
            angles()
        if k == 5:
            took(xblk(on_x(0, 1 - c)), xs.at[4], xr.at[4])
            for d in (0, 1):
                took(xblk(on_x(-SIDES[d], 1 - c)), xs.at[5 + d], xr.at[5 + d])
            took(xblk(on_x(2, 1 - c)), xs.at[7], xr.at[7])
            normalise()
            project(WB, accb, 3, 1)
        if k == 6:
            for j in (2, 3, 4, 5):
                project(WB, accb, 3, j)
        if k == 7:
            for j in (6, 7):
                project(WB, accb, 3, j)
    for i, o in origins(8):
        y_onward(WA, o, *ya(i), AROWS)
    project(WB, accb, 3, 0)
    states()
    spread_states()
    for k in range(0, 9):
        for i, o in origins(k):
            y_last(WA, o, *ya(i), AROWS)
    for k in (1, 2, 3, 4, 5, 6, 7, 0):
        project(WA, acca, 4, k)
    halo_send()
    spread_rows()
    for k in range(9):
        turn_output(k)
    attend()
    convolve()
    return_rows()
    finish()
    reduce_out()
    for cp in sent:
        cp.wait_send()


def mixer(tok, gain, outer, inner, conv, query, key, value, gate, taps, decay, head_gain, conv_o, ret_o):
    dma = pltpu.SemaphoreType.DMA
    vm, anywhere = pl.BlockSpec(memory_space=pltpu.VMEM), pl.BlockSpec(memory_space=pl.ANY)
    return pl.pallas_call(
        mixer_kernel,
        out_shape=jax.ShapeDtypeStruct((64, 2048), BF),
        in_specs=[anywhere, vm] + [anywhere] * 7 + [vm] * 5,
        out_specs=vm,
        scratch_shapes=[
            pltpu.VMEM((16, SPAN, 128), BF),
            pltpu.VMEM((16, SPAN, 128), BF),
            pltpu.VMEM((NZ, NY, AROWS, 128), BF),
            pltpu.VMEM((NZ, NY, BROWS, 128), BF),
            pltpu.VMEM((256, 2048), BF),
            pltpu.VMEM((3, SPAN, 128), F32),
            pltpu.VMEM((4, SPAN, 128), F32),
            pltpu.VMEM((2, SPAN, SPAN), F32),
            pltpu.VMEM((4, SPAN, 128), F32),
            pltpu.VMEM((2, SPAN, 128), F32),
            pltpu.VMEM((3, SPAN, 128), BF),
            pltpu.VMEM((SPAN, 512), F32),
            pltpu.VMEM((SPAN, 256), BF),
            pltpu.VMEM((2, 8, 128), F32),
            pltpu.VMEM((2, 8, 128), F32),
            pltpu.VMEM((NY, 40, 128), F32),
            pltpu.VMEM((NY, 40, 128), F32),
            pltpu.VMEM((2, 24, 128), F32),
            pltpu.VMEM((NZ, 24, 128), F32),
            pltpu.VMEM((NY, 32, 128), BF),
            pltpu.VMEM((NY, 32, 128), BF),
            pltpu.VMEM((NX, 2, 2, 64, 1024), BF),
            pltpu.VMEM((NX, 2, 64, 1024), BF),
            pltpu.VMEM((NX, 2, 64, 1024), BF),
            pltpu.VMEM((2, 64, 1024), BF),
            pltpu.VMEM((2, 2, 64, 1024), BF),
            dma((9,)),
            dma((2, 8)), dma((2, 8)), dma((2, 8, 4)), dma((2, 8, 4)),
            dma((4, 16)), dma((4, 16)), dma((4,)), dma((4,)), dma((8,)), dma((8,)),
            dma((2,)), dma((2,)), dma((3,)), dma((3,)), dma((16,)), dma((16,)), dma((3,)), dma((3,)),
            dma((4,)), dma((4,)), dma((2,)), dma((2,)), dma((2, 2)), dma((2, 2)),
        ],
        compiler_params=pltpu.CompilerParams(
            collective_id=0, has_side_effects=True, vmem_limit_bytes=56 * 1024 * 1024
        ),
    )(
        tok, gain.reshape(16, 128), outer, inner, conv, query, key, value, gate, taps, decay,
        head_gain.reshape(1, 128), conv_o.T, ret_o.T,
    )


def solution(mesh):
    return jax.shard_map(
        mixer,
        mesh=mesh,
        in_specs=(
            P("sp", "tp"),
            P(),
            P("sp", "tp"),
            P("sp", "tp"),
            P("sp", "tp"),
            P("sp", "tp"),
            P("sp", "tp"),
            P("sp", "tp"),
            P("sp", "tp"),
            P(None, "tp"),
            P(None, "tp", "sp"),
            P("tp"),
            P("tp", "sp"),
            P("tp", "sp"),
        ),
        out_specs=P(("sp", "tp"), None),
        check_vma=False,
    )
```

time: 287 us -> 99.7 us (0.35)
  waiting for transfers between devices: 104 us -> 0 us
  Pallas kernels: 52.5 us -> 97.8 us
  blocking collectives: 40.1 us -> 0 us
  matrix products: 24 us -> 0 us
  local copies, waits for them, and re-layouts: 25.6 us -> 1.67 us
  starting transfers between devices: 14.8 us -> 0 us
  between operations: 13.7 us -> 0.01 us
  other arithmetic: 11.1 us -> 0 us
    all_gather x1 -> x0, waiting for transfers between devices: 104 us -> none  [in_one_piece(): lax.all_gather(both, axis, axis=dim, tiled=True)]
    pallas_call x1, Pallas kernels: 52.5 us -> 97.8 us  [mixer(): pl.pallas_call(mixer_kernel, out_shape=jax.ShapeDtypeStruct((64, 2048), B...]
    all_to_all x1 -> x0, blocking collectives: 40.1 us -> none  [sum_at_owner(): lax.all_to_all(parts, axis, split_axis=0, concat_axis=0, tiled=True)]
    dot_general x14 -> x0, matrix products: 24 us -> none  [the longest x1 5.87 us: local(): jnp.dot(ret_out, ret_weight, preferred_element_type=jnp.float32)]
    all_to_all x1 -> x0, starting transfers between devices: 10.4 us -> none  [from_everyone(): return lax.all_to_all(copies, axis, split_axis=0, concat_axis=0, tiled=True)]
    unnamed x46 -> x1, local copies, waits for them, and re-layouts: 7.79 us -> 1.67 us
    slice x11 -> x0, local copies, waits for them, and re-layouts: 5.83 us -> none  [the longest x2 4.61 us: local(): pick = lambda a, i: a[:, i].reshape(2048, 128)]
    split x1 -> x0, local copies, waits for them, and re-layouts: 4.96 us -> none  [in_one_piece(): jnp.split(lax.all_gather(both, axis, axis=dim, tiled=True), ends, axis=al...]
  transfers between devices with their start and end apart: 4 -> 0, of which waited for: 1 -> 0; matrix products, arithmetic and copies ran while one was open for 7% -> 0% of each run, Pallas kernels for 0% -> 0%
where the time goes in v2:
time: 99.7 us; the launch traced here: 99.5 us
  Pallas kernels  97.8 us (98%)
  local copies, waits for them, and re-layouts  1.67 us (2%)
    pallas_call x1, Pallas kernels, mixer(): pl.pallas_call(mixer_kernel, out_shape=jax.ShapeDtypeStruct((64, 2048), B...  97.8 us

profile of v2, /device:TPU:1, one launch (start us, length us, event | category | flops | bytes accessed | tf_op | source)
XLA Modules:
  0.0 99.5 jit_solution(10243293209446687832)
XLA Ops:
  0.0 97.8 %shard_map.136 = bf16[64,2048]{1,0:T(8,128)(2,1)} custom-call(bf16[512,256]{1,0:T(8,128)(2,1)} %tok.1, f32[16,128]{1,0:T(8,128)} %bitcast.4, bf16[32,128]{1,0:T(8,128)(2,1)} %outer_w.1, bf16[32,128]{1,0:T(8,128)(2,1)} %inner_w.1, bf16[32,128]{1,0:T(8,128)(2,1)} %conv_w.1, bf16[32,128]{1,0:T(8,128)(2,1)} %query_w.1, bf16[32,128]{1,0:T(8,128)(2,1)} %key_w.1, ...), custom_call_target="tpu_custom_call" | custom-call | tf_op jit(solution)/shard_map/pallas_call | solution.py:481
  97.8 1.7 %copy.16 = bf16[64,2048]{1,0:T(8,128)(2,1)} copy(bf16[64,2048]{1,0:T(8,128)(2,1)} %shard_map.136) | data formatting | bytes 524288

commit v3 on v2

v3 whole, which is shorter than its diff:
```python
import math

import jax
import jax.numpy as jnp
from jax import lax
from jax.experimental import pallas as pl
from jax.experimental.pallas import tpu as pltpu
from jax.sharding import PartitionSpec as P

NZ, NY, NX = 16, 4, 4
SPAN, HEAD = 512, 64
EPS, THETA = 1e-06, 10000.0
KROWS, BROWS, AROWS = 64, 96, 128
MESH = pl.DeviceIdType.MESH
BF, F32 = jnp.bfloat16, jnp.float32
SIDES = (1, -1)


def ring(value, step, size):
    return lax.rem(value + (step + size), size)


def rows_of(i, n):
    return pl.ds(pl.multiple_of(i * n, n), n)


def nn(a, b):
    return lax.dot_general(a, b, (((1,), (0,)), ((), ())), preferred_element_type=F32)


def nt(a, b):
    return lax.dot_general(a, b, (((1,), (1,)), ((), ())), preferred_element_type=F32)


def tn(a, b):
    return lax.dot_general(a, b, (((0,), (0,)), ((), ())), preferred_element_type=F32)


def left_head(shape):
    return lax.broadcasted_iota(jnp.int32, shape, len(shape) - 1) < HEAD


def mixer_kernel(
    tok, gain_in, outer_w, inner_w, conv_w, query_w, key_w, value_w, gate_w, taps_in, decay_in, head_gain_in, conv_o, ret_o,
    out,
    gain, taps, decay, head_gain, X, NR, WK, WA, WB, WO, acck, accb, acca, D, scale, trig, qkv, mix, CR, halo_s, halo_r,
    msg_a, got_a, msg_b, got_b, msg_c, got_c, part, pair, quads, via, fin, done,
    loc, kzr, kyr, zar, zbr, yar, yahr, ybr, xr, hr, sar, sbr, scr, dr, vr, fr, ssem, outs,
):
    s, t = lax.axis_index("sp"), lax.axis_index("tp")
    z, y, x, c = s // NY, lax.rem(s, NY), t // 2, lax.rem(t, 2)

    def at(dz=0, dy=0, dx=0, dc=0):
        return (ring(z, dz, NZ) * NY + ring(y, dy, NY), ring(x, dx, NX) * 2 + ring(c, dc, 2))

    def push(src, dst, sem, rsem, dev):
        pltpu.make_async_remote_copy(
            src_ref=src, dst_ref=dst, send_sem=ssem.at[sem], recv_sem=rsem, device_id=dev, device_id_type=MESH
        ).start()

    def all_left(ref, sem):
        pltpu.make_async_remote_copy(
            src_ref=ref, dst_ref=ref, send_sem=ssem.at[sem], recv_sem=kyr.at[0], device_id=at(dz=1), device_id_type=MESH
        ).wait_send()

    def took(ref, rsem):
        pltpu.make_async_remote_copy(
            src_ref=ref, dst_ref=ref, send_sem=ssem.at[0], recv_sem=rsem, device_id=at(dz=1), device_id_type=MESH
        ).wait_recv()

    barrier = pltpu.get_barrier_semaphore()
    near = [at(dz=1), at(dz=-1), at(dz=2), at(dz=-2), at(dy=1), at(dy=-1), at(dy=2), at(dx=1), at(dx=-1), at(dc=1)]
    for d in near:
        pl.semaphore_signal(barrier, inc=1, device_id=d, device_id_type=MESH)
    moves = [(w, WK.at[z, y, pl.ds(32 * i, 32)]) for i, w in enumerate((key_w, value_w))]
    moves += [(w, WB.at[z, y, pl.ds(32 * i, 32)]) for i, w in enumerate((query_w, inner_w, conv_w))]
    moves += [(w, WA.at[z, y, pl.ds(32 * i, 32)]) for i, w in enumerate((gate_w, outer_w, conv_o, ret_o))]
    moves += [(tok.at[:, pl.ds(128 * i, 128)], X.at[2 * t + i]) for i in (0, 1)]
    moves += [(gain_in, gain), (taps_in, taps), (decay_in, decay), (head_gain_in, head_gain)]
    own = [pltpu.make_async_copy(a, b, loc.at[i]) for i, (a, b) in enumerate(moves)]
    for o in own:
        o.start()

    def own_here():
        for o in own:
            o.wait()

    def greeted():
        pl.semaphore_wait(barrier, len(near))

    def half_or_all(k, d, rows):
        return pl.ds(0, rows) if k < 8 else pl.ds(d * (rows // 2), rows // 2)

    def send_kv(k):
        for d in (0, 1):
            back = (k - 1) // 2 * 2
            ref = WK.at[ring(z, -SIDES[d] * back, NZ), y, half_or_all(k, d, KROWS)]
            push(ref, ref, 0, kzr.at[d, k - 1], at(dz=SIDES[d] * (k - back)))

    def recv_kv(k):
        for d in (0, 1):
            took(WK.at[ring(z, -SIDES[d] * k, NZ), y, half_or_all(k, d, KROWS)], kzr.at[d, k - 1])

    def y_kv(k):
        for _, o in origins(k):
            for dy in (2, 1, 3):
                push(WK.at[o, y], WK.at[o, y], 1, kyr.at[0], at(dy=dy))

    def send_za(k):
        for d in (0, 1):
            ref = WA.at[ring(z, -SIDES[d] * (k - 1), NZ), y, half_or_all(k, d, AROWS)]
            push(ref, ref, 2, zar.at[d, k - 1], at(dz=SIDES[d]))

    def recv_za(k):
        for d in (0, 1):
            took(WA.at[ring(z, -SIDES[d] * k, NZ), y, half_or_all(k, d, AROWS)], zar.at[d, k - 1])

    def send_zb(k, j):
        for d in (0, 1):
            ref = WB.at[ring(z, -SIDES[d] * (k - 1), NZ), ring(y, j, NY), half_or_all(k, d, BROWS)]
            push(ref, ref, 3, zbr.at[d, k - 1, j], at(dz=SIDES[d]))

    def recv_zb(k, j):
        for d in (0, 1):
            ref = WB.at[ring(z, -SIDES[d] * k, NZ), ring(y, j, NY), half_or_all(k, d, BROWS)]
            took(ref, zbr.at[d, k - 1, j])

    def side(d, rows):
        return pl.ds(d * (rows // 2), rows // 2)

    def ya_direct(k):
        for i, o in origins(k):
            for d in (0, 1):
                push(WA.at[o, y], WA.at[o, y], 4, yar.at[d, i], at(dy=SIDES[d]))

    def ya_onward(k):
        for i, o in origins(k):
            for d in (0, 1):
                src = ring(y, -SIDES[d], NY)
                took(WA.at[o, src], yar.at[d, i])
                ref = WA.at[o, src, side(d, AROWS)]
                push(ref, ref, 4, yahr.at[0 if k < 6 else 1], at(dy=SIDES[d]))

    def yb_direct():
        for dy in (2, 1, 3):
            push(WB.at[z, y], WB.at[z, y], 5, ybr.at[dy - 1], at(dy=dy))

    def yb_take(j):
        took(WB.at[z, ring(y, j, NY)], ybr.at[NY - 1 - j])

    def origins(k):
        if k == 0:
            return [(0, z)]
        if k == 8:
            return [(15, ring(z, 8, NZ))]
        return [(k, ring(z, -k, NZ)), (7 + k, ring(z, k, NZ))]

    def xblk(tt, half=None):
        return X.at[pl.ds(2 * tt, 2)] if half is None else X.at[2 * tt + half]

    def on_x(dx, core):
        return ring(x, dx, NX) * 2 + core

    def xpush(tt, half, i, dev):
        push(xblk(tt, half), xblk(tt, half), 6, xr.at[i], dev)

    def x_start():
        for d in (0, 1):
            for h in (d, 1 - d):
                xpush(t, h, 2 * d + h, at(dx=SIDES[d]))

    def x_onward():
        for d in (0, 1):
            src = on_x(-SIDES[d], c)
            took(xblk(src, d), xr.at[3 * d])
            xpush(src, d, 4 + d, at(dx=SIDES[d]))

    def x_partner():
        for d in (0, 1):
            src = on_x(-SIDES[d], c)
            took(xblk(src, 1 - d), xr.at[2 * d + 1 - d])
            xpush(src, None, 7 + d, at(dc=1))

    def x_far():
        for d in (0, 1):
            took(xblk(on_x(2, c), d), xr.at[4 + d])
        xpush(on_x(2, c), None, 9, at(dc=1))

    def x_all():
        took(xblk(on_x(0, 1 - c)), xr.at[6])
        for d in (0, 1):
            took(xblk(on_x(-SIDES[d], 1 - c)), xr.at[7 + d])
        took(xblk(on_x(2, 1 - c)), xr.at[9])

    def decay_sums():
        row = lax.broadcasted_iota(jnp.int32, (SPAN, SPAN), 0)
        col = lax.broadcasted_iota(jnp.int32, (SPAN, SPAN), 1)
        lower = jnp.where(col <= row, 1.0, 0.0).astype(BF)
        upper = jnp.where(col >= row, 1.0, 0.0).astype(BF)
        for i, (tri, turned) in enumerate(((lower, upper), (upper, lower))):
            rest = jnp.concatenate([jnp.broadcast_to(decay[i, h : h + 1, :], (128, SPAN)) for h in (0, 1)], axis=0)
            over, along = None, None
            for _ in range(3):
                term = rest.astype(BF)
                rest = rest - term.astype(F32)
                o, a = nt(tri, term), nn(jnp.concatenate([term[0:8], term[128:136]], axis=0), turned)
                over, along = (o, a) if over is None else (over + o, along + a)
            mix[pl.ds(16 * i, 16), :] = along
            for h in (0, 1):
                scale[2 * i + h] = over[:, 128 * h : 128 * h + 128]

    def decay_matrix(h):
        row = lax.broadcasted_iota(jnp.int32, (128, SPAN), 0)
        col = lax.broadcasted_iota(jnp.int32, (128, SPAN), 1)

        def chunk(i, _):
            wide = lambda a: jnp.concatenate([a] * 4, axis=1)
            cf = wide(scale[h, rows_of(i, 128)]) - mix[pl.ds(8 * h, 1), :]
            rb = wide(scale[2 + h, rows_of(i, 128)]) - mix[pl.ds(16 + 8 * h, 1), :]
            D[h, rows_of(i, 128)] = jnp.exp(jnp.where(col <= row + i * 128, cf, rb))
            return 0

        lax.fori_loop(0, 4, chunk, 0)

    def decay_scales():
        left = left_head((SPAN, 128))
        cf = jnp.where(left, scale[0], scale[1])
        rb = jnp.where(left, scale[2], scale[3])
        scale[0] = jnp.exp(cf)
        scale[1] = jnp.exp(rb)
        scale[2] = jnp.exp(cf[SPAN - 1 : SPAN] - cf)
        scale[3] = jnp.exp(rb[0:1] - rb)
        tot = jnp.where(lax.broadcasted_iota(jnp.int32, (8, 128), 0) == 0, cf[SPAN - 1 : SPAN], rb[0:1])
        for q in range(NY):
            msg_a[q, pl.ds(32, 8)] = tot

    def angles():
        def chunk(i, _):
            lane = lax.broadcasted_iota(jnp.int32, (128, 128), 1)
            pos = (lax.broadcasted_iota(jnp.int32, (128, 128), 0) + (s * SPAN + i * 128)).astype(F32)
            freq = jnp.exp(-math.log(THETA) * lax.rem(lane, 32).astype(F32) * (2.0 / HEAD))
            ang = pos * freq
            trig[0, rows_of(i, 128)] = jnp.cos(ang)
            sine = jnp.sin(ang)
            trig[1, rows_of(i, 128)] = jnp.where(lax.rem(lane, HEAD) < HEAD // 2, -sine, sine)
            return 0

        lax.fori_loop(0, 4, chunk, 0)

    def normalise():
        def chunk(i, _):
            r = rows_of(i, 64)
            total = jnp.zeros((64, 128), F32)
            for b in range(16):
                w = X[b, r].astype(F32)
                total = total + w * w
            inv = lax.rsqrt(jnp.sum(total, axis=1, keepdims=True) * (1.0 / 2048) + EPS)
            for b in range(16):
                NR[b, r] = (X[b, r].astype(F32) * inv * gain[pl.ds(b, 1), :]).astype(BF)
            return 0

        lax.fori_loop(0, 8, chunk, 0)

    def project_kv():
        def chunk(i, _):
            r = rows_of(i, 256)
            lhs = jnp.concatenate([NR[b, r] for b in range(NZ)], axis=1)
            w = [WK[:, :, pl.ds(32 * n, 32), :].reshape(2048, 128) for n in (0, 1)]
            both = nn(lhs, jnp.concatenate(w, axis=1))
            acck[0, r] = both[:, :128]
            acck[1, r] = both[:, 128:]
            return 0

        lax.fori_loop(0, 2, chunk, 0)

    def project_part(buf, acc, count, base, hops, first):
        os = [o for k in hops for _, o in origins(k)]
        lhs = jnp.concatenate([NR[o] for o in os], axis=1)
        for n in range(0, count):
            w = jnp.concatenate([buf[o, :, pl.ds(base + 32 * n, 32), :].reshape(128, 128) for o in os], axis=0)
            total = nn(lhs, w)
            acc[n] = total if first else acc[n] + total

    def project_b(*hops):
        project_part(WB, accb, 3, 0, hops, hops[0] == 1)

    def project_a(*hops):
        project_part(WA, acca, 2, 0, hops, hops[0] == 0)

    def turn_output(k):
        for _, o in origins(k):
            for i in (0, 1):
                w = WA[o, :, pl.ds(64 + 32 * i, 32), :].reshape(128, 128)
                WO[pl.ds(128 * i, 128), pl.ds(pl.multiple_of(o * 128, 128), 128)] = w.T

    def rotated(a):
        wide = a.astype(BF).astype(F32)
        first = lax.rem(lax.broadcasted_iota(jnp.int32, wide.shape, 1), HEAD) < HEAD // 2
        other = jnp.where(first, pltpu.roll(wide, 96, axis=1), pltpu.roll(wide, 32, axis=1))
        return wide * trig[0] + other * trig[1]

    def states():
        rk = (rotated(acck[0]) * HEAD**-0.5).astype(BF)
        value = acck[1].astype(BF)
        qkv[1] = rk
        qkv[2] = value
        wide = rk.astype(F32)
        left = left_head((HEAD, 128))
        for i in (0, 1):
            full = tn((wide * scale[2 + i]).astype(BF), value)
            packed = jnp.where(left, full[0:HEAD], full[HEAD:])
            for q in range(NY):
                msg_a[q, pl.ds(16 * i, 16)] = packed[16 * q : 16 * q + 16]

    def attend():
        qkv[0] = rotated(accb[0]).astype(BF)
        rk, value = qkv[1], qkv[2]

        def chunk(i, _):
            r = rows_of(i, 128)
            rq = qkv[0, r]
            left = left_head((128, 128))
            zero = jnp.zeros_like(rq)
            parts = []
            for h, own_q in enumerate((jnp.where(left, rq, zero), jnp.where(left, zero, rq))):
                probs = (nt(own_q, rk) * D[h, r]).astype(BF)
                parts.append(nn(probs, value))
            mix[r, pl.ds(0, 128)] = jnp.where(left, parts[0], parts[1])
            return 0

        lax.fori_loop(0, 4, chunk, 0, unroll=True)

    def inner_value():
        return (accb[1].astype(BF).astype(F32) * accb[2].astype(BF).astype(F32)).astype(BF).astype(F32)

    def halo_send():
        inner = inner_value()
        halo_s[0] = inner[0:8]
        halo_s[1] = inner[SPAN - 8 :]
        push(halo_s.at[1], halo_r.at[0], 7, hr.at[0], (lax.rem(s + 1, NZ * NY), t))
        push(halo_s.at[0], halo_r.at[1], 7, hr.at[1], (lax.rem(s + NZ * NY - 1, NZ * NY), t))

    def convolve():
        for i in (0, 1):
            took(halo_r.at[i], hr.at[i])
        inner = inner_value()
        row = lax.broadcasted_iota(jnp.int32, (SPAN, 128), 0)
        before = jnp.where(s == 0, 0.0, halo_r[0, 7:8, :])
        after = jnp.where(s == NZ * NY - 1, 0.0, halo_r[1, 0:1, :])
        prev = jnp.where(row == 0, before, pltpu.roll(inner, 1, axis=0))
        follow = jnp.where(row == SPAN - 1, after, pltpu.roll(inner, SPAN - 1, axis=0))
        conv = taps[0:1, :] * prev + taps[1:2, :] * inner + taps[2:3, :] * follow
        CR[:, pl.ds(0, 128)] = (acca[1].astype(BF).astype(F32) * conv).astype(BF)

    def spread_states():
        for dy in (1, 2, 3):
            yy = ring(y, dy, NY)
            push(msg_a.at[yy], got_a.at[y], 8, sar.at[dy - 1], at(dy=dy))
        got_a[y] = msg_a[y]

    def step_terms():
        return [
            (got_a[m, pl.ds(0, 16)], got_a[m, pl.ds(16, 16)], jnp.exp(got_a[m, pl.ds(32, 1)]), jnp.exp(got_a[m, pl.ds(33, 1)]))
            for m in range(NY)
        ]

    def spread_rows():
        for dy in (1, 2, 3):
            took(got_a.at[ring(y, -dy, NY)], sar.at[dy - 1])
        terms = step_terms()
        fwd, bwd = terms[0][0], terms[NY - 1][1]
        for m in range(1, NY):
            fwd = terms[m][2] * fwd + terms[m][0]
            back = terms[NY - 1 - m]
            bwd = back[3] * bwd + back[1]
        msg_b[0, pl.ds(0, 16)] = fwd
        msg_b[1, pl.ds(0, 16)] = bwd
        for i in (0, 1):
            total = got_a[0, pl.ds(32 + i, 1)]
            for m in range(1, NY):
                total = total + got_a[m, pl.ds(32 + i, 1)]
            msg_b[i, pl.ds(16, 8)] = jnp.broadcast_to(total, (8, 128))
        for d in (8, 7, 9, 6, 10, 5, 11, 4, 12, 3, 13, 2, 14, 1, 15):
            push(msg_b.at[(z + d) // NZ], got_b.at[d], 9, sbr.at[d], at(dz=d))

    def return_rows():
        for d in range(1, NZ):
            took(got_b.at[d], sbr.at[d])
        fwd = jnp.zeros((16, 128), F32)
        bwd = jnp.zeros((16, 128), F32)
        for d in range(NZ - 1, 0, -1):
            lower = jnp.exp(got_b[d, pl.ds(16, 1)]) * fwd + got_b[d, pl.ds(0, 16)]
            fwd = jnp.where(d <= z, lower, fwd)
            e = NZ - d
            higher = jnp.exp(got_b[e, pl.ds(16, 1)]) * bwd + got_b[e, pl.ds(0, 16)]
            bwd = jnp.where(d <= NZ - 1 - z, higher, bwd)
        terms = step_terms()
        for m in range(NY):
            msg_c[m, pl.ds(0, 16)] = fwd.astype(BF)
            fwd = terms[m][2] * fwd + terms[m][0]
            n = NY - 1 - m
            msg_c[n, pl.ds(16, 16)] = bwd.astype(BF)
            bwd = terms[n][3] * bwd + terms[n][1]
        for dy in (2, 1, 3):
            yy = ring(y, dy, NY)
            push(msg_c.at[yy], got_c.at[y], 10, scr.at[dy - 1], at(dy=dy))
        got_c[y] = msg_c[y]

    def finish():
        for dy in (1, 2, 3):
            took(got_c.at[ring(y, -dy, NY)], scr.at[dy - 1])
        left = left_head((HEAD, 128))
        into = []
        for i in (0, 1):
            packed = jnp.concatenate([got_c[q, pl.ds(16 * i, 16)] for q in range(NY)], axis=0)
            zero = jnp.zeros_like(packed)
            into.append(jnp.concatenate([jnp.where(left, packed, zero), jnp.where(left, zero, packed)], axis=0))
        both = jnp.concatenate(into, axis=1)
        same = (
            (lax.broadcasted_iota(jnp.int32, (128, 128), 0) < HEAD) == (lax.broadcasted_iota(jnp.int32, (128, 128), 1) < HEAD)
        ).astype(F32) * (1.0 / HEAD)
        same = same.astype(BF)

        def chunk(i, _):
            r = rows_of(i, 128)
            carried = nn(qkv[0, r], both)
            m = mix[r, pl.ds(0, 128)] + scale[0, r] * carried[:, :128] + scale[1, r] * carried[:, 128:]
            square = m * m
            high = square.astype(BF)
            inv = lax.rsqrt(nn(high, same) + nn((square - high.astype(F32)).astype(BF), same) + EPS)
            g = acca[0, r].astype(BF).astype(F32)
            silu = g / (1.0 + jnp.exp(-g))
            CR[r, pl.ds(128, 128)] = (silu * (m * inv * head_gain[...])).astype(BF)
            return 0

        lax.fori_loop(0, 4, chunk, 0)

    def out_rows(xo):
        rows = CR[rows_of(ring(x, xo, NX), 128)]
        for h in (0, 1):
            for n in (0, 1):
                res = nn(rows, WO[:, pl.ds(1024 * h + 512 * n, 512)]).astype(BF).reshape(2, 64, 512)
                part[xo, :, h, :, pl.ds(512 * n, 512)] = res
            push(part.at[xo, 1 - c, h], pair.at[xo, h], 11, dr.at[xo, h], at(dc=1))

    def summed(xo, half):
        took(pair.at[xo, half], dr.at[xo, half])
        return part[xo, c, half].astype(F32) + pair[xo, half].astype(F32)

    def far_out():
        for h in (0, 1):
            quads[2, h] = summed(2, h).astype(BF)
            push(quads.at[2, h], via.at[h], 12, vr.at[h], at(dx=SIDES[h]))

    def near_out():
        for xo, d in ((1, 0), (3, 1)):
            quads[xo, 1 - d] = summed(xo, 1 - d).astype(BF)
            push(quads.at[xo, 1 - d], fin.at[d, 1 - d], 13, fr.at[d, 1 - d], at(dx=SIDES[d]))

    def last_out():
        sums = [summed(xo, d) for xo, d in ((1, 0), (3, 1))]
        for xo, d in ((1, 0), (3, 1)):
            took(via.at[d], vr.at[d])
            quads[xo, d] = (sums[d] + via[d].astype(F32)).astype(BF)
            push(quads.at[xo, d], fin.at[d, d], 13, fr.at[d, d], at(dx=SIDES[d]))

    def own_out():
        for h in (0, 1):
            total = summed(0, h)
            for d in (1 - h, h):
                took(fin.at[d, h], fr.at[d, h])
                total = total + fin[d, h].astype(F32)
            done[:, pl.ds(1024 * h, 1024)] = total.astype(BF)
            pltpu.make_async_copy(done.at[:, pl.ds(1024 * h, 1024)], out.at[:, pl.ds(1024 * h, 1024)], outs.at[h]).start()

    def leave():
        all_left(WK.at[pl.ds(0, 15), 0], 0)
        all_left(WK.at[pl.ds(0, 12)], 1)
        all_left(WA.at[pl.ds(0, 15), 0], 2)
        all_left(WB.at[pl.ds(0, 15)], 3)
        all_left(WA.at[pl.ds(0, 12)], 4)
        all_left(WB.at[0, pl.ds(0, 3)], 5)
        all_left(X.at[pl.ds(0, 14)], 6)
        all_left(halo_s, 7)
        all_left(msg_a.at[pl.ds(0, 3)], 8)
        all_left(got_b.at[pl.ds(0, 15)], 9)
        all_left(msg_c.at[pl.ds(0, 3)], 10)
        all_left(pair, 11)
        all_left(via, 12)
        all_left(fin, 13)
        for h in (0, 1):
            cols = pl.ds(1024 * h, 1024)
            pltpu.make_async_copy(done.at[:, cols], out.at[:, cols], outs.at[h]).wait()

    own_here()
    greeted()
    send_kv(1)
    send_kv(2)
    yb_direct()
    send_zb(1, 0)
    y_kv(0)
    x_start()
    send_za(1)
    ya_direct(0)
    xpush(t, None, 6, at(dc=1))
    decay_sums()
    for k in range(1, 9):
        if k <= 4:
            recv_kv(2 * k)
            if k < 4:
                send_kv(2 * k + 1)
                send_kv(2 * k + 2)
            y_kv(2 * k)
            recv_kv(2 * k - 1)
            y_kv(2 * k - 1)
        if k == 1:
            for j in (1, 3, 2):
                yb_take(j)
                send_zb(1, j)
        recv_za(k)
        if k < 8:
            send_za(k + 1)
        ya_direct(k)
        if k == 2:
            x_onward()
        for j in (0, 1, 3, 2):
            recv_zb(k, j)
            if k < 8:
                send_zb(k + 1, j)
        ya_onward(k - 1)
        if k == 1:
            decay_matrix(0)
        if k == 2:
            decay_matrix(1)
            decay_scales()
            x_partner()
        if k == 3:
            angles()
            x_far()
        if k == 4:
            x_all()
            normalise()
        if k == 5:
            took(WK.at[pl.ds(0, 12)], kyr.at[0])
            project_kv()
            states()
            spread_states()
        if k == 6:
            project_b(1, 2, 3)
        if k == 7:
            spread_rows()
            project_b(4, 5)
        if k == 8:
            project_b(6, 7)
            took(WA.at[pl.ds(0, 11), 0], yahr.at[0])
    ya_onward(8)
    project_b(0, 8)
    halo_send()
    return_rows()
    attend()
    project_a(0, 1, 2, 3, 4, 5)
    for k in range(0, 6):
        turn_output(k)
    took(WA.at[pl.ds(0, 5), 0], yahr.at[1])
    project_a(6, 7, 8)
    for k in range(6, 9):
        turn_output(k)
    convolve()
    finish()
    for xo in (2, 1, 3):
        out_rows(xo)
    far_out()
    near_out()
    out_rows(0)
    last_out()
    own_out()
    leave()


def mixer(tok, gain, outer, inner, conv, query, key, value, gate, taps, decay, head_gain, conv_o, ret_o):
    dma = pltpu.SemaphoreType.DMA
    anywhere = pl.BlockSpec(memory_space=pl.ANY)
    return pl.pallas_call(
        mixer_kernel,
        out_shape=jax.ShapeDtypeStruct((64, 2048), BF),
        in_specs=[anywhere] * 14,
        out_specs=anywhere,
        scratch_shapes=[
            pltpu.VMEM((16, 128), F32),
            pltpu.VMEM((3, 128), F32),
            pltpu.VMEM((2, 2, SPAN), F32),
            pltpu.VMEM((1, 128), F32),
            pltpu.VMEM((16, SPAN, 128), BF),
            pltpu.VMEM((16, SPAN, 128), BF),
            pltpu.VMEM((NZ, NY, KROWS, 128), BF),
            pltpu.VMEM((NZ, NY, AROWS, 128), BF),
            pltpu.VMEM((NZ, NY, BROWS, 128), BF),
            pltpu.VMEM((256, 2048), BF),
            pltpu.VMEM((2, SPAN, 128), F32),
            pltpu.VMEM((3, SPAN, 128), F32),
            pltpu.VMEM((2, SPAN, 128), F32),
            pltpu.VMEM((2, SPAN, SPAN), F32),
            pltpu.VMEM((4, SPAN, 128), F32),
            pltpu.VMEM((2, SPAN, 128), F32),
            pltpu.VMEM((3, SPAN, 128), BF),
            pltpu.VMEM((SPAN, 512), F32),
            pltpu.VMEM((SPAN, 256), BF),
            pltpu.VMEM((2, 8, 128), F32),
            pltpu.VMEM((2, 8, 128), F32),
            pltpu.VMEM((NY, 40, 128), F32),
            pltpu.VMEM((NY, 40, 128), F32),
            pltpu.VMEM((2, 24, 128), F32),
            pltpu.VMEM((NZ, 24, 128), F32),
            pltpu.VMEM((NY, 32, 128), BF),
            pltpu.VMEM((NY, 32, 128), BF),
            pltpu.VMEM((NX, 2, 2, 64, 1024), BF),
            pltpu.VMEM((NX, 2, 64, 1024), BF),
            pltpu.VMEM((NX, 2, 64, 1024), BF),
            pltpu.VMEM((2, 64, 1024), BF),
            pltpu.VMEM((2, 2, 64, 1024), BF),
            pltpu.VMEM((64, 2048), BF),
            dma((15,)), dma((2, 8)), dma((1,)), dma((2, 8)), dma((2, 8, 4)), dma((2, 16)), dma((2,)), dma((3,)),
            dma((10,)), dma((2,)), dma((3,)), dma((16,)), dma((3,)), dma((4, 2)), dma((2,)), dma((2, 2)), dma((14,)),
            dma((2,)),
        ],
        compiler_params=pltpu.CompilerParams(
            collective_id=0, has_side_effects=True, vmem_limit_bytes=56 * 1024 * 1024
        ),
    )(
        tok, gain.reshape(16, 128), outer, inner, conv, query, key, value, gate, taps, decay,
        head_gain.reshape(1, 128), conv_o.T, ret_o.T,
    )


def solution(mesh):
    return jax.shard_map(
        mixer,
        mesh=mesh,
        in_specs=(
            P("sp", "tp"),
            P(),
            P("sp", "tp"),
            P("sp", "tp"),
            P("sp", "tp"),
            P("sp", "tp"),
            P("sp", "tp"),
            P("sp", "tp"),
            P("sp", "tp"),
            P(None, "tp"),
            P(None, "tp", "sp"),
            P("tp"),
            P("tp", "sp"),
            P("tp", "sp"),
        ),
        out_specs=P(("sp", "tp"), None),
        check_vma=False,
    )
```

time: 99.7 us -> 78.7 us (0.79)
  Pallas kernels: 97.8 us -> 76.9 us
    pallas_call x1, Pallas kernels: 97.8 us -> 76.9 us  [mixer(): pl.pallas_call(mixer_kernel, out_shape=jax.ShapeDtypeStruct((64, 2048), B...]
where the time goes in v3:
time: 78.7 us; the launch traced here: 78.6 us
  Pallas kernels  76.9 us (98%)
  local copies, waits for them, and re-layouts  1.67 us (2%)
    pallas_call x1, Pallas kernels, mixer(): pl.pallas_call(mixer_kernel, out_shape=jax.ShapeDtypeStruct((64, 2048), B...  76.9 us
    unnamed x1, local copies, waits for them, and re-layouts  1.67 us

profile of v3, /device:TPU:1, one launch (start us, length us, event | category | flops | bytes accessed | tf_op | source)
XLA Modules:
  0.0 78.6 jit_solution(18046500209305736571)
XLA Ops:
  0.0 76.9 %shard_map.136 = bf16[64,2048]{1,0:T(8,128)(2,1)} custom-call(bf16[512,256]{1,0:T(8,128)(2,1)} %tok.1, f32[16,128]{1,0:T(8,128)} %bitcast.4, bf16[32,128]{1,0:T(8,128)(2,1)} %outer_w.1, bf16[32,128]{1,0:T(8,128)(2,1)} %inner_w.1, bf16[32,128]{1,0:T(8,128)(2,1)} %conv_w.1, bf16[32,128]{1,0:T(8,128)(2,1)} %query_w.1, bf16[32,128]{1,0:T(8,128)(2,1)} %key_w.1, ...), custom_call_target="tpu_custom_call" | custom-call | tf_op jit(solution)/shard_map/pallas_call | solution.py:583
  76.9 1.7 %copy.16 = bf16[64,2048]{1,0:T(8,128)(2,1)} copy(bf16[64,2048]{1,0:T(8,128)(2,1)} %shard_map.136) | data formatting | bytes 524288
